TPU v7x, 32 devices: a whole 2x2x4 slice. The times are simulated.
32 devices in a mesh: grp: 2 (over y), sp: 4 (over z), tp: 4 (over x, core).
Axes of the slice: x: 2, y: 2, z: 4, core: 2. Of those that a mesh axis runs over, the one named last changes fastest.
Arguments:
- hidden_in: bfloat16 [2048, 2048], P(('grp', 'sp')), parts along dimension 0, may hold values from -6 to 6
- query_latent_rows: bfloat16 [2048, 768], P(('grp', 'sp')), parts along dimension 0, may hold values from -6 to 6
- key_value_latent: bfloat16 [2048, 512], P(('grp', 'sp')), parts along dimension 0, may hold values from -6 to 6
- rotary_key: bfloat16 [2048, 32], P(('grp', 'sp')), parts along dimension 0, may hold values from -64 to 64
- query_norm_gain: float32 [768], replicated, may hold values from 0.1 to 1.9
- key_value_gain: float32 [512], replicated, may hold values from 0.1 to 1.9
- query_up_weight: bfloat16 [768, 1536], P(None, 'tp'), may hold values from -0.625 to 0.625
- key_value_up_weight: bfloat16 [512, 2048], P(None, 'tp'), may hold values from -0.25 to 0.25
- out_proj: bfloat16 [1024, 2048], P('tp'), may hold values from -0.1875 to 0.1875
- feed_gain: float32 [2048], replicated, may hold values from 0.1 to 1.9
- feed_up: bfloat16 [2048, 8192], P('sp', 'tp'), may hold values from -0.125 to 0.125
- feed_down: bfloat16 [8192, 2048], P('tp', 'sp'), may hold values from -0.0625 to 0.0625
Outputs:
- layer_out: bfloat16 [2048, 2048], P(('grp', 'sp', 'tp')), parts along dimension 0
There are 2 independent parts, one for each index of `grp`. A program takes and returns all parts, laid end to end along the dimension named above; an argument that names none is the same for every part. Nothing has to cross between parts.
All inputs are finite; a program needn't handle non-finite values.
Results may differ from a plain program's by a relative error of at most 0.02.
Values may be sent and summed in bfloat16 or wider, within the bound.
A program may use at most 128 MiB of HBM per device.

v0:
```python
import math

import jax
import jax.numpy as jnp
from jax import lax
from jax.experimental import pallas as pl
from jax.experimental.pallas import tpu as pltpu
from jax.sharding import PartitionSpec as P

QUERY_KEY_PLAIN = 64
QUERY_KEY_ROTARY = 32
VALUE_HEAD_SIZE = 64


def normalize(values, gain):
    floats = values.astype(jnp.float32)
    return floats * lax.rsqrt(jnp.mean(floats * floats, axis=-1, keepdims=True) + 1e-06) * gain


def rotate(values, position):
    half_size = values.shape[-1] // 2
    inverse = 10000.0 ** (-jnp.arange(half_size, dtype=jnp.float32) * 2.0 / values.shape[-1])
    angles = position[:, None] * inverse[None, :]
    cosine = jnp.concatenate([jnp.cos(angles), jnp.cos(angles)], axis=-1)
    sine = jnp.concatenate([jnp.sin(angles), jnp.sin(angles)], axis=-1)
    shape = (values.shape[0],) + (1,) * (values.ndim - 2) + (values.shape[-1],)
    turned = jnp.concatenate([-values[..., half_size:], values[..., :half_size]], axis=-1)
    return values * cosine.reshape(shape) + turned * sine.reshape(shape)


MESH = pl.DeviceIdType.MESH


def layer_kernel(
    n, heads, qp, qr, lat, wkv, hidden, op, gain, up, down, out,
    lat_all, kv_all, op_pad, mixed, up_all, down_all, part_d, recv_d, middle, norm_all, act, part,
    rf1, c2, rf2, c3, rf3, ss, rs, ls,
):
    g, me, t = lax.axis_index("grp"), lax.axis_index("sp"), lax.axis_index("tp")
    c, x = lax.rem(t, 2), t // 2
    share, width = middle.shape
    rows = share * 4
    rank = wkv.shape[0]
    piece_k = up.shape[0]
    hid = down_all.shape[0]
    half_k, half_h = piece_k // 2, hid // 2
    wide = down.shape[1]
    scale_factor = (QUERY_KEY_PLAIN + QUERY_KEY_ROTARY) ** (-0.5)

    def at_z(k):
        return lax.rem(me + k, n)

    def from_z(k):
        return lax.rem(me - k + n, n)

    def at_tp(cc, xx):
        return {"tp": xx * 2 + cc}

    sib, xpeer, ypeer = at_tp(1 - c, x), at_tp(c, 1 - x), {"grp": 1 - g}
    barrier = pltpu.get_barrier_semaphore()
    for k in range(1, n):
        pl.semaphore_signal(barrier, inc=1, device_id={"sp": at_z(k)}, device_id_type=MESH)
    for peer in (sib, xpeer, at_tp(1 - c, 1 - x), ypeer):
        pl.semaphore_signal(barrier, inc=1, device_id=peer, device_id_type=MESH)
    pl.semaphore_wait(barrier, n + 3)

    names = {}
    sent = []

    def slot(name):
        if name not in names:
            names[name] = len(names)
        return names[name]

    def send(name, src, dst, dev):
        i = slot(name)
        copy = pltpu.make_async_remote_copy(
            src_ref=src, dst_ref=dst, send_sem=ss.at[i], recv_sem=rs.at[i],
            device_id=dev, device_id_type=MESH,
        )
        copy.start()
        sent.append(copy)

    def land(name, dst):
        i = slot(name)
        pltpu.make_async_remote_copy(
            src_ref=dst, dst_ref=dst, send_sem=ss.at[i], recv_sem=rs.at[i],
            device_id=sib, device_id_type=MESH,
        ).wait_recv()

    def up_half(owner, hv):
        return up_all.at[pl.ds(pl.multiple_of(owner * piece_k + hv * half_k, half_k), half_k)]

    def down_half(owner, hv):
        return down_all.at[
            pl.ds(pl.multiple_of(hv * half_h, half_h), half_h),
            pl.ds(pl.multiple_of(owner * wide, wide), wide),
        ]

    def begin(tag, buf):
        own = buf.at[me, c, x]
        for k in range(1, n):
            send((tag, "z", k), own, own, {"sp": at_z(k)})
        send((tag, "x", 0), own, own, xpeer)
        send((tag, "s", 0), own, own, sib)

    def finish(tag, buf):
        for k in range(1, n):
            piece = buf.at[from_z(k), c, x]
            land((tag, "z", k), piece)
            send((tag, "x", k), piece, piece, xpeer)
            send((tag, "s", k), piece, piece, sib)
        for k in range(n):
            piece = buf.at[from_z(k), c, 1 - x]
            land((tag, "x", k), piece)
            send((tag, "t", k), piece, piece, sib)
        for k in range(n):
            land((tag, "s", k), buf.at[from_z(k), 1 - c, x])
            land((tag, "t", k), buf.at[from_z(k), 1 - c, 1 - x])

    def send_down(k):
        send(
            ("dn", k),
            down.at[pl.ds(pl.multiple_of(at_z(k) * hid + g * half_h, half_h), half_h)],
            down_half(me, g),
            {"sp": at_z(k)},
        )

    lat_all[me, c, x] = lat[...]
    begin("l", lat_all)
    for k in range(1, n):
        send(
            ("up", k),
            up.at[
                pl.ds(pl.multiple_of(g * half_k, half_k), half_k),
                pl.ds(pl.multiple_of(at_z(k) * hid, hid), hid),
            ],
            up_half(me, g),
            {"sp": at_z(k)},
        )
    for k in range(1, n):
        send_down(k)
    local = [
        pltpu.make_async_copy(
            up.at[:, pl.ds(pl.multiple_of(me * hid, hid), hid)],
            up_all.at[pl.ds(pl.multiple_of(me * piece_k, piece_k), piece_k)],
            ls.at[0],
        ),
        pltpu.make_async_copy(
            down.at[pl.ds(pl.multiple_of(me * hid, hid), hid)],
            down_all.at[:, pl.ds(pl.multiple_of(me * wide, wide), wide)],
            ls.at[1],
        ),
    ]
    for copy in local:
        copy.start()
    vh = VALUE_HEAD_SIZE
    unit = QUERY_KEY_PLAIN + vh
    for h in range(heads):
        op_pad[h * unit : h * unit + QUERY_KEY_PLAIN] = jnp.zeros((QUERY_KEY_PLAIN, width), op.dtype)
        op_pad[h * unit + QUERY_KEY_PLAIN : (h + 1) * unit] = op[h * vh : (h + 1) * vh]
    finish("l", lat_all)
    for j in range(n):
        kv_all[j] = jnp.dot(
            lat_all[j, :, :, :, :rank].reshape(rows, rank),
            wkv[...],
            preferred_element_type=jnp.float32,
        ).astype(jnp.bfloat16)

    contract = (((1,), (1,)), ((), ()))
    rope = lat_all[:, :, :, :, rank:].reshape(n * rows, -1)
    for h in range(heads):
        kv = kv_all[:, :, h * unit : (h + 1) * unit].reshape(n * rows, unit)
        scores = lax.dot_general(qp[h], kv, contract, preferred_element_type=jnp.float32)
        scores += lax.dot_general(qr[h], rope, contract, preferred_element_type=jnp.float32)
        scores = scores * scale_factor
        expo = jnp.exp(scores - jnp.max(scores, axis=-1, keepdims=True))
        total = jnp.sum(expo, axis=-1, keepdims=True)
        mix = jnp.dot(expo.astype(jnp.bfloat16), kv, preferred_element_type=jnp.float32)
        mixed[:, h * unit : (h + 1) * unit] = (mix / total).astype(jnp.bfloat16)

    tile = math.gcd(width, 512)

    @pl.loop(0, width // tile)
    def _(j):
        cols = pl.ds(pl.multiple_of(j * tile, tile), tile)
        part_d[:, cols] = jnp.dot(
            mixed[...], op_pad[:, cols], preferred_element_type=jnp.float32
        ).astype(jnp.bfloat16)

    def own_rows(cc, xx):
        return pl.ds(pl.multiple_of((xx * 2 + cc) * share, share), share)

    others = ((c, 1 - x), (1 - c, 1 - x), (1 - c, x))
    for j, (cc, xx) in enumerate(others):
        send(("d", j), part_d.at[own_rows(cc, xx)], recv_d.at[j], at_tp(cc, xx))
    branch = part_d[own_rows(c, x)].astype(jnp.float32)
    for j in range(3):
        land(("d", j), recv_d.at[j])
        branch += recv_d[j].astype(jnp.float32)
    middle[...] = (hidden[own_rows(c, x)].astype(jnp.float32) + branch).astype(jnp.bfloat16)
    norm_all[me, c, x] = normalize(middle[...], gain[...]).astype(jnp.bfloat16)

    begin("n", norm_all)
    for k in range(1, n):
        piece = up_half(from_z(k), g)
        land(("up", k), piece)
        send(("uy", k), piece, piece, ypeer)
    for k in range(1, n):
        piece = down_half(from_z(k), g)
        land(("dn", k), piece)
        send(("dy", k), piece, piece, ypeer)
    finish("n", norm_all)
    for k in range(1, n):
        land(("uy", k), up_half(from_z(k), 1 - g))
    local[0].wait()
    @pl.loop(0, n)
    def _(j):
        upward = jnp.dot(
            norm_all[j].reshape(rows, width), up_all[...], preferred_element_type=jnp.float32
        )
        act[j] = jnp.square(jnp.maximum(upward, 0.0)).astype(jnp.bfloat16)

    for k in range(1, n):
        land(("dy", k), down_half(from_z(k), 1 - g))
    local[1].wait()

    order = [*range(1, n), 0]
    for k in order:
        dest = at_z(k)

        @pl.loop(0, width // tile)
        def _(j):
            cols = pl.ds(pl.multiple_of(j * tile, tile), tile)
            made = jnp.dot(act[dest], down_all[:, cols], preferred_element_type=jnp.float32)
            part[k, :, :, :, cols] = made.astype(jnp.bfloat16).reshape(2, 2, share, tile)

        send(("f1", k), part.at[k, 1 - c], rf1.at[k], sib)
    for k in order:
        land(("f1", k), rf1.at[k])
        c2[k] = (
            part[k, c, 1 - x].astype(jnp.float32) + rf1[k, 1 - x].astype(jnp.float32)
        ).astype(jnp.bfloat16)
        send(("f2", k), c2.at[k], rf2.at[k], xpeer)
    for k in order:
        land(("f2", k), rf2.at[k])
        c3[k] = (
            part[k, c, x].astype(jnp.float32)
            + rf1[k, x].astype(jnp.float32)
            + rf2[k].astype(jnp.float32)
        ).astype(jnp.bfloat16)
        if k:
            send(("f3", k), c3.at[k], rf3.at[k], {"sp": at_z(k)})
    feed = c3[0].astype(jnp.float32)
    for k in range(1, n):
        land(("f3", k), rf3.at[k])
        feed += rf3[k].astype(jnp.float32)
    out[...] = (middle[...].astype(jnp.float32) + feed).astype(jnp.bfloat16)
    for copy in sent:
        copy.wait_send()


def run_layer(
    queries, latent, key_rope, key_value_up_weight, hidden_in, out_proj, feed_gain, feed_up, feed_down
):
    n = lax.axis_size("sp")
    rows, heads, size = queries.shape
    width = hidden_in.shape[1]
    share = rows // lax.axis_size("tp")
    hid = feed_up.shape[1] // n
    turned = jnp.transpose(queries, (1, 0, 2))
    unit = QUERY_KEY_PLAIN + VALUE_HEAD_SIZE
    plain = jnp.pad(turned[..., :QUERY_KEY_PLAIN], ((0, 0), (0, 0), (0, VALUE_HEAD_SIZE)))
    rotary = jnp.pad(turned[..., QUERY_KEY_PLAIN:], ((0, 0), (0, 0), (0, unit - QUERY_KEY_ROTARY)))
    lat = jnp.concatenate(
        [latent, jnp.pad(key_rope, ((0, 0), (0, unit - QUERY_KEY_ROTARY)))], axis=1
    )
    lat = lax.dynamic_slice_in_dim(lat, lax.axis_index("tp") * share, share, 0)
    bf = jnp.bfloat16
    vmem = pl.BlockSpec(memory_space=pltpu.VMEM)
    anywhere = pl.BlockSpec(memory_space=pl.ANY)
    copies = 16 * n
    block = (share, width)
    return pl.pallas_call(
        lambda *refs: layer_kernel(n, heads, *refs),
        out_shape=jax.ShapeDtypeStruct(block, bf),
        in_specs=[vmem] * 7 + [anywhere] * 2,
        out_specs=vmem,
        scratch_shapes=[
            pltpu.VMEM((n, 2, 2, *lat.shape), bf),
            pltpu.VMEM((n, rows, heads * unit), bf),
            pltpu.VMEM((heads * unit, width), bf),
            pltpu.VMEM((rows, heads * unit), bf),
            pltpu.VMEM((feed_up.shape[0] * n, hid), bf),
            pltpu.VMEM((hid, feed_down.shape[1] * n), bf),
            pltpu.VMEM((rows, width), bf),
            pltpu.VMEM((3, *block), bf),
            pltpu.VMEM(block, bf),
            pltpu.VMEM((n, 2, 2, *block), bf),
            pltpu.VMEM((n, rows, hid), bf),
            pltpu.VMEM((n, 2, 2, *block), bf),
            pltpu.VMEM((n, 2, *block), bf),
            pltpu.VMEM((n, *block), bf),
            pltpu.VMEM((n, *block), bf),
            pltpu.VMEM((n, *block), bf),
            pltpu.VMEM((n, *block), bf),
            pltpu.SemaphoreType.DMA((copies,)),
            pltpu.SemaphoreType.DMA((copies,)),
            pltpu.SemaphoreType.DMA((2,)),
        ],
        compiler_params=pltpu.CompilerParams(
            collective_id=0, has_side_effects=True, vmem_limit_bytes=60 * 1024 * 1024
        ),
    )(
        plain, rotary, lat, key_value_up_weight, hidden_in, out_proj,
        feed_gain.reshape(1, -1), feed_up, feed_down,
    )


def fits_kernel(tokens, feed_up):
    n = lax.axis_size("sp")
    hid = feed_up.shape[1] // n
    return (
        lax.axis_size("grp") == 2
        and lax.axis_size("tp") == 4
        and 1 < n
        and tokens * n <= 1024
        and tokens % 64 == 0
        and hid % 128 == 0
        and hid <= 512
    )


def on_device(
    hidden_in,
    query_latent_rows,
    key_value_latent,
    rotary_key,
    query_norm_gain,
    key_value_gain,
    query_up_weight,
    key_value_up_weight,
    out_proj,
    feed_gain,
    feed_up,
    feed_down,
):
    tokens_here = hidden_in.shape[0]
    heads_here = query_up_weight.shape[1] // (QUERY_KEY_PLAIN + QUERY_KEY_ROTARY)
    position = (lax.axis_index("sp") * tokens_here + jnp.arange(tokens_here)).astype(jnp.float32)
    scale_factor = (QUERY_KEY_PLAIN + QUERY_KEY_ROTARY) ** (-0.5)
    query_norm = normalize(query_latent_rows, query_norm_gain).astype(jnp.bfloat16)
    queries = jnp.dot(query_norm, query_up_weight, preferred_element_type=jnp.float32).reshape(
        tokens_here, heads_here, QUERY_KEY_PLAIN + QUERY_KEY_ROTARY
    )
    queries = jnp.concatenate(
        [queries[..., :QUERY_KEY_PLAIN], rotate(queries[..., QUERY_KEY_PLAIN:], position)], axis=-1
    ).astype(jnp.bfloat16)
    query_plain = queries[..., :QUERY_KEY_PLAIN]
    query_turned = queries[..., QUERY_KEY_PLAIN:]
    latent = normalize(key_value_latent, key_value_gain).astype(jnp.bfloat16)
    key_rope = rotate(rotary_key.astype(jnp.float32), position).astype(jnp.bfloat16)

    def attend_block(carry, key_plain, value_rows, rope_rows):
        row_max, denom, accum = carry
        scores = jnp.einsum(
            "qhd,khd->hqk", query_plain, key_plain, preferred_element_type=jnp.float32
        )
        scores = scores + jnp.einsum(
            "qhd,kd->hqk", query_turned, rope_rows, preferred_element_type=jnp.float32
        )
        scores = scores * scale_factor
        new_max = jnp.maximum(row_max, jnp.max(scores, axis=-1))
        expo = jnp.exp(scores - new_max[:, :, None])
        factor = jnp.exp(row_max - new_max)
        denom = denom * factor + jnp.sum(expo, axis=-1)
        update = jnp.einsum(
            "hqk,khd->qhd",
            expo.astype(jnp.bfloat16),
            value_rows,
            preferred_element_type=jnp.float32,
        )
        accum = accum * jnp.transpose(factor)[:, :, None] + update
        return (new_max, denom, accum)

    start_carry = (
        jnp.full((heads_here, tokens_here), -1e30, jnp.float32),
        jnp.zeros((heads_here, tokens_here), jnp.float32),
        jnp.zeros((tokens_here, heads_here, VALUE_HEAD_SIZE), jnp.float32),
    )
    own_keys = jnp.dot(latent, key_value_up_weight, preferred_element_type=jnp.float32).astype(
        jnp.bfloat16
    )
    if fits_kernel(tokens_here, feed_up):
        return run_layer(
            queries, latent, key_rope, key_value_up_weight, hidden_in, out_proj,
            feed_gain, feed_up, feed_down,
        )
    pieces = (
        lax.all_gather(own_keys, "sp", axis=0, tiled=True),
        lax.all_gather(key_rope, "sp", axis=0, tiled=True),
    )
    rows_in = pieces[0].shape[0]
    block = math.gcd(rows_in, 1024)

    def step_block(index, inner):
        first = index * block
        bulk = lax.dynamic_slice_in_dim(pieces[0], first, block, 0)
        rope_rows = lax.dynamic_slice_in_dim(pieces[1], first, block, 0)
        bulk = bulk.reshape(block, heads_here, QUERY_KEY_PLAIN + VALUE_HEAD_SIZE)
        return attend_block(
            inner, bulk[..., :QUERY_KEY_PLAIN], bulk[..., QUERY_KEY_PLAIN:], rope_rows
        )

    final_carry = lax.fori_loop(0, rows_in // block, step_block, start_carry)
    denom = final_carry[1]
    accum = final_carry[2]
    mixed = (
        (accum / jnp.transpose(denom)[:, :, None])
        .astype(jnp.bfloat16)
        .reshape(tokens_here, heads_here * VALUE_HEAD_SIZE)
    )
    up_own = lax.all_to_all(feed_up, "sp", split_axis=1, concat_axis=0, tiled=True)
    down_own = lax.all_to_all(feed_down, "sp", split_axis=0, concat_axis=1, tiled=True)
    share = tokens_here // lax.axis_size("tp")
    lead = lax.axis_index("tp") * share
    branch = lax.psum_scatter(
        jnp.dot(mixed, out_proj, preferred_element_type=jnp.float32).astype(jnp.bfloat16),
        "tp",
        scatter_dimension=0,
        tiled=True,
    ).astype(jnp.float32)
    hidden_own = lax.dynamic_slice_in_dim(hidden_in, lead, share, 0)
    middle_own = (hidden_own.astype(jnp.float32) + branch).astype(jnp.bfloat16)
    normed_own = normalize(middle_own, feed_gain).astype(jnp.bfloat16)
    normed = lax.all_gather(normed_own, ("sp", "tp"), axis=0, tiled=True)
    upward = jnp.dot(normed, up_own, preferred_element_type=jnp.float32)
    activated = jnp.square(jax.nn.relu(upward)).astype(jnp.bfloat16)
    partial_sum = jnp.dot(activated, down_own, preferred_element_type=jnp.float32)
    feed = lax.psum_scatter(
        partial_sum.astype(jnp.bfloat16), ("sp", "tp"), scatter_dimension=0, tiled=True
    ).astype(jnp.float32)
    return (middle_own.astype(jnp.float32) + feed).astype(jnp.bfloat16)


def solution(mesh):
    return jax.shard_map(
        on_device,
        mesh=mesh,
        in_specs=(
            P(("grp", "sp"), None),
            P(("grp", "sp"), None),
            P(("grp", "sp"), None),
            P(("grp", "sp"), None),
            P(),
            P(),
            P(None, "tp"),
            P(None, "tp"),
            P("tp", None),
            P(),
            P("sp", "tp"),
            P("tp", "sp"),
        ),
        out_specs=P(("grp", "sp", "tp"), None),
        check_vma=False,
    )
```

profile of v0, /device:TPU:8, one launch (start us, length us, event | category | flops | bytes accessed | tf_op | source)
XLA Modules:
  0.0 145.7 jit_solution(7020414858195453051)
XLA Ops:
  0.0 0.0 copy-start
  0.0 0.0 copy-start.2
  0.0 0.0 copy-start.1
  0.0 0.0 copy-start.4
  0.0 0.0 copy-start.3
  0.1 1.2 fusion
  1.3 1.1 fusion.3
  2.4 0.1 multiply_cosine_fusion
  2.6 0.7 fusion.14
  3.3 0.1 copy.44
  3.4 0.1 copy.49
  3.5 0.1 copy.45
  3.6 0.1 copy.50
  3.7 0.8 copy.47
  4.5 0.1 fusion.12
  4.6 0.0 copy-done.2
  4.7 0.0 copy-done.4
  4.7 0.1 fusion.5
  4.8 0.7 fusion.13.refs_2_
  5.5 0.0 copy-done
  5.5 0.0 copy-done.1
  5.5 0.0 copy-done.3
  5.5 0.4 fusion.6
  6.0 0.2 copy.53
  6.2 0.2 copy.46
  6.4 0.2 copy.54
  6.6 0.1 add_convert_fusion
  6.7 0.1 maximum_bitcast_fusion
  6.8 0.8 pad.12.refs_0_
  7.6 0.1 slice.40
  7.7 0.7 pad.13.refs_1_
  8.5 135.5 %shard_map.118 = bf16[64,2048]{1,0:T(8,128)(2,1)} custom-call(bf16[4,256,128]{2,1,0:T(8,128)(2,1)} %pad.12.refs_0_, bf16[4,256,128]{2,1,0:T(8,128)(2,1)} %pad.13.refs_1_, bf16[64,640]{1,0:T(8,128)(2,1)} %fusion.13.refs_2_, bf16[512,512]{1,0:T(8,128)(2,1)} %refs_3_.1, bf16[256,2048]{1,0:T(8,128)(2,1)} %refs_4_.1, bf16[256,2048]{1,0:T(8,128)(2,1)} %refs_5_.1, ...), custom_call_target="tpu_custom_call" | custom-call | tf_op jit(solution)/shard_map/pallas_call | solution.py:284
  144.0 1.7 %copy.56 = bf16[64,2048]{1,0:T(8,128)(2,1)} copy(bf16[64,2048]{1,0:T(8,128)(2,1)} %shard_map.118) | data formatting | bytes 524288
  (10 shorter events, 0.1 us)
Async XLA Ops:
  0.0 5.5 %copy-start = (bf16[768,384]{1,0:T(8,128)(2,1)S(1)}, bf16[768,384]{1,0:T(8,128)(2,1)}, u32[]{:S(2)}) copy-start(bf16[768,384]{1,0:T(8,128)(2,1)} %param.18) | copy-start | bytes 1769476
  0.0 4.6 %copy-start.2 = (bf16[256,512]{1,0:T(8,128)(2,1)S(1)}, bf16[256,512]{1,0:T(8,128)(2,1)}, u32[]{:S(2)}) copy-start(bf16[256,512]{1,0:T(8,128)(2,1)} %param.14) | copy-start | bytes 786436
  0.0 5.5 %copy-start.1 = (bf16[256,768]{1,0:T(8,128)(2,1)S(1)}, bf16[256,768]{1,0:T(8,128)(2,1)}, u32[]{:S(2)}) copy-start(bf16[256,768]{1,0:T(8,128)(2,1)} %param.13) | copy-start | bytes 1179652
  0.0 4.6 %copy-start.4 = (f32[512]{0:T(512)S(1)}, f32[512]{0:T(512)}, u32[]{:S(2)}) copy-start(f32[512]{0:T(512)} %param.17) | copy-start | bytes 6148
  0.0 5.4 %copy-start.3 = (f32[768]{0:T(1024)S(1)}, f32[768]{0:T(1024)}, u32[]{:S(2)}) copy-start(f32[768]{0:T(1024)} %param.16) | copy-start | bytes 9220
where the time goes:
time: 146 us
  Pallas kernels  136 us (93%)
  local copies, waits for them, and re-layouts  5.85 us (4%)
  other arithmetic  3.65 us (2%)
    pallas_call x1, Pallas kernels, run_layer(): pl.pallas_call(lambda *refs: layer_kernel(n, heads, *refs), out_shape=jax...  136 us

commit v1 on v0

v1 whole, which is shorter than its diff:
```python
import math

import jax
import jax.numpy as jnp
import numpy as np
from jax import lax
from jax.experimental import pallas as pl
from jax.experimental.pallas import tpu as pltpu
from jax.sharding import PartitionSpec as P

QUERY_KEY_PLAIN = 64
QUERY_KEY_ROTARY = 32
VALUE_HEAD_SIZE = 64


def normalize(values, gain):
    floats = values.astype(jnp.float32)
    return floats * lax.rsqrt(jnp.mean(floats * floats, axis=-1, keepdims=True) + 1e-06) * gain


def rotate(values, position):
    half_size = values.shape[-1] // 2
    inverse = 10000.0 ** (-jnp.arange(half_size, dtype=jnp.float32) * 2.0 / values.shape[-1])
    angles = position[:, None] * inverse[None, :]
    cosine = jnp.concatenate([jnp.cos(angles), jnp.cos(angles)], axis=-1)
    sine = jnp.concatenate([jnp.sin(angles), jnp.sin(angles)], axis=-1)
    shape = (values.shape[0],) + (1,) * (values.ndim - 2) + (values.shape[-1],)
    turned = jnp.concatenate([-values[..., half_size:], values[..., :half_size]], axis=-1)
    return values * cosine.reshape(shape) + turned * sine.reshape(shape)


MESH = pl.DeviceIdType.MESH


def layer_kernel(
    n, heads, table, kvlat, rk, qlat, gq, gkv, gain, turn, perm, wq, wkv, hidden, op, up, down, out,
    lat_in, rk_in, q_in, wq_in, wkv_in, perm_in, hid_in,
    lat_all, kv_all, q_all, op_all, mixed, mixed_in, up_all, down_all, middle, norm_all, act, part,
    rf1, c2, rf2, c3, rf3, ss, rs, ls,
):
    g, me, t = lax.axis_index("grp"), lax.axis_index("sp"), lax.axis_index("tp")
    c, x = lax.rem(t, 2), t // 2
    share, width = middle.shape
    rows = share * 4
    rank = wkv.shape[0]
    piece_k = up.shape[0]
    hid = down_all.shape[0]
    half_k, half_h = piece_k // 2, hid // 2
    wide = down.shape[1]
    bf, f32 = jnp.bfloat16, jnp.float32
    vh = VALUE_HEAD_SIZE
    unit = QUERY_KEY_PLAIN + vh
    lanes = heads * QUERY_KEY_ROTARY
    scale_factor = (QUERY_KEY_PLAIN + QUERY_KEY_ROTARY) ** (-0.5)
    inner = jnp.minimum(me, n - 1 - me)

    def near(i):
        if i == 0:
            return me
        step = (i + 1) // 2
        turned = me - step if i % 2 else me + step
        return jnp.where(i <= 2 * inner, turned, jnp.where(2 * me < n - 1, i, n - 1 - i))

    def at_tp(cc, xx):
        return {"tp": xx * 2 + cc}

    sib, xpeer, ypeer = at_tp(1 - c, x), at_tp(c, 1 - x), {"grp": 1 - g}
    barrier = pltpu.get_barrier_semaphore()
    for i in range(1, n):
        pl.semaphore_signal(barrier, inc=1, device_id={"sp": near(i)}, device_id_type=MESH)
    for peer in (sib, xpeer, at_tp(1 - c, 1 - x), ypeer):
        pl.semaphore_signal(barrier, inc=1, device_id=peer, device_id_type=MESH)

    def rows_of(tt):
        return pl.ds(pl.multiple_of(tt * share, share), share)

    mine = rows_of(t)
    local = []

    def fetch(src, dst):
        copy = pltpu.make_async_copy(src, dst, ls.at[len(local)])
        copy.start()
        local.append(copy)
        return copy

    got_lat = fetch(kvlat.at[mine], lat_in)
    got_rk = fetch(rk.at[mine], rk_in)
    got_perm = fetch(perm, perm_in)
    got_wq = fetch(wq, wq_in)
    got_q = fetch(qlat, q_in)
    got_wkv = fetch(wkv, wkv_in)
    op_rows = op.shape[0]
    got_op = fetch(op, op_all.at[pl.ds(pl.multiple_of(t * op_rows, op_rows), op_rows)])
    got_hid = fetch(hidden.at[mine], hid_in)
    got_up = fetch(
        up.at[:, pl.ds(pl.multiple_of(me * hid, hid), hid)],
        up_all.at[pl.ds(pl.multiple_of(me * piece_k, piece_k), piece_k)],
    )
    got_down = fetch(
        down.at[pl.ds(pl.multiple_of(me * hid, hid), hid)],
        down_all.at[:, pl.ds(pl.multiple_of(me * wide, wide), wide)],
    )

    names = {}
    sent = []

    def slot(name, at):
        if name not in names:
            names[name] = sum(size for _, size in names.values()), 1 if at is None else n
        return names[name][0] + (0 if at is None else at)

    def send(name, src, dst, dev, to=None, by=None):
        copy = pltpu.make_async_remote_copy(
            src_ref=src, dst_ref=dst, send_sem=ss.at[slot(name, to)], recv_sem=rs.at[slot(name, by)],
            device_id=dev, device_id_type=MESH,
        )
        copy.start()
        sent.append(copy)

    def land(name, dst, by=None):
        pltpu.make_async_remote_copy(
            src_ref=dst, dst_ref=dst, send_sem=ss.at[slot(name, by)], recv_sem=rs.at[slot(name, by)],
            device_id=sib, device_id_type=MESH,
        ).wait_recv()

    def up_half(owner, hv):
        return up_all.at[pl.ds(pl.multiple_of(owner * piece_k + hv * half_k, half_k), half_k)]

    def down_half(owner, hv):
        return down_all.at[
            pl.ds(pl.multiple_of(hv * half_h, half_h), half_h),
            pl.ds(pl.multiple_of(owner * wide, wide), wide),
        ]

    def begin(tag, buf):
        own = buf.at[me, c, x]
        send((tag, "x"), own, own, xpeer, me, me)
        for i in reversed(range(1, n)):
            send((tag, "z"), own, own, {"sp": near(i)}, near(i), me)
        send((tag, "s"), own, own, sib, me, me)

    def relay(tag, buf, i):
        z = near(i)
        piece = buf.at[z, c, x]
        land((tag, "z"), piece, z)
        send((tag, "x"), piece, piece, xpeer, z, z)
        send((tag, "s"), piece, piece, sib, z, z)

    def cross(tag, buf, i):
        z = near(i)
        piece = buf.at[z, c, 1 - x]
        land((tag, "x"), piece, z)
        send((tag, "t"), piece, piece, sib, z, z)

    def settle(tag, buf, i):
        z = near(i)
        land((tag, "s"), buf.at[z, 1 - c, x], z)
        land((tag, "t"), buf.at[z, 1 - c, 1 - x], z)

    got_lat.wait()
    got_rk.wait()
    lat_all[me, c, x, :, :rank] = normalize(lat_in[...], gkv[...]).astype(bf)
    spun = jnp.dot(rk_in[...], turn[...], preferred_element_type=f32)
    lat_all[me, c, x, :, rank:] = (
        spun[:, :lanes] * table[0, mine, :] + spun[:, lanes:] * table[1, mine, :]
    ).astype(bf)
    pl.semaphore_wait(barrier, n + 3)
    begin("l", lat_all)
    for i in reversed(range(1, n)):
        send(
            "up",
            up.at[
                pl.ds(pl.multiple_of(g * half_k, half_k), half_k),
                pl.ds(pl.multiple_of(near(i) * hid, hid), hid),
            ],
            up_half(me, g),
            {"sp": near(i)},
            near(i),
            me,
        )

    op_parts = 4
    op_piece = op_rows // op_parts

    def op_block(tt, j):
        return op_all.at[pl.ds(pl.multiple_of(tt * op_rows + j * op_piece, op_piece), op_piece)]

    def send_op(j):
        own = op_block(t, j)
        send(("ox", j), own, own, xpeer)

    got_op.wait()
    send_op(0)
    own_op = op_all.at[pl.ds(pl.multiple_of(t * op_rows, op_rows), op_rows)]
    send("os", own_op, own_op, sib)

    got_perm.wait()
    got_wq.wait()
    wide_q = jnp.dot(wq_in[...], perm_in[...], preferred_element_type=f32).astype(bf)
    got_q.wait()
    query_norm = normalize(q_in[...], gq[...]).astype(bf)
    spread = jnp.dot(query_norm, wide_q, preferred_element_type=f32)
    first = heads * unit
    spin = (
        spread[:, first : first + lanes] * table[0] + spread[:, first + lanes : first + 2 * lanes] * table[1]
    )
    lane = lax.broadcasted_iota(jnp.int32, (rows, lanes), 1)
    for h in range(heads):
        q_all[h, :, :unit] = spread[:, h * unit : (h + 1) * unit].astype(bf)
        keep = (lane >= h * QUERY_KEY_ROTARY) & (lane < (h + 1) * QUERY_KEY_ROTARY)
        q_all[h, :, unit:] = jnp.where(keep, spin, 0.0).astype(bf)

    for i in range(1, n):
        relay("l", lat_all, i)
    for j in range(1, op_parts):
        send_op(j)
    got_wkv.wait()
    for i in range(n):
        cross("l", lat_all, i)
    for i in range(n):
        settle("l", lat_all, i)
    for j in range(n):
        made = jnp.dot(
            lat_all[j, :, :, :, :rank].reshape(rows, rank), wkv_in[...], preferred_element_type=f32
        ).astype(bf)
        rope = lat_all[j, :, :, :, rank:].reshape(rows, lanes)
        for h in range(heads):
            kv_all[h, j * rows : (j + 1) * rows, :unit] = made[:, h * unit : (h + 1) * unit]
            kv_all[h, j * rows : (j + 1) * rows, unit:] = rope

    contract = (((1,), (1,)), ((), ()))
    low = lax.broadcasted_iota(jnp.int32, (rows, unit), 1) < vh

    def attend(h):
        scores = lax.dot_general(q_all[h], kv_all[h], contract, preferred_element_type=f32)
        scores = scores * scale_factor
        expo = jnp.exp(scores - jnp.max(scores, axis=-1, keepdims=True))
        total = jnp.sum(expo, axis=-1, keepdims=True)
        mix = jnp.dot(expo.astype(bf), kv_all[h, :, :unit], preferred_element_type=f32)
        return mix / total

    others = ((c, 1 - x), (1 - c, 1 - x), (1 - c, x))
    for p in range(heads // 2):
        left, right = attend(2 * p), attend(2 * p + 1)
        pair = jnp.where(low, pltpu.roll(left, vh, 1), right)
        mixed[p] = pair.astype(bf)
        cols = pl.ds(pl.multiple_of(t * heads * vh + p * unit, unit), unit)
        for j, (cc, xx) in enumerate(others):
            send(
                ("m", p, j), mixed.at[p, rows_of(xx * 2 + cc)], mixed_in.at[:, cols], at_tp(cc, xx)
            )
        mixed_in[:, cols] = mixed[p, mine, :]

    for j in range(op_parts):
        piece = op_block((1 - x) * 2 + c, j)
        land(("ox", j), piece)
        send(("ot", j), piece, piece, sib)
    for i in range(1, n):
        piece = up_half(near(i), g)
        land("up", piece, near(i))
        send("uy", piece, piece, ypeer, near(i), near(i))
    land("os", op_all.at[pl.ds(pl.multiple_of((x * 2 + 1 - c) * op_rows, op_rows), op_rows)])
    for j in range(op_parts):
        land(("ot", j), op_block((1 - x) * 2 + 1 - c, j))
    for p in range(heads // 2):
        for j, (cc, xx) in enumerate(others):
            cols = pl.ds(pl.multiple_of((xx * 2 + cc) * heads * vh + p * unit, unit), unit)
            land(("m", p, j), mixed_in.at[:, cols])

    tile = math.gcd(width, 512)
    got_hid.wait()

    @pl.loop(0, width // tile)
    def _(j):
        cols = pl.ds(pl.multiple_of(j * tile, tile), tile)
        branch = jnp.dot(mixed_in[...], op_all[:, cols], preferred_element_type=f32)
        middle[:, cols] = (hid_in[:, cols].astype(f32) + branch).astype(bf)

    norm_all[me, c, x] = normalize(middle[...], gain[...]).astype(bf)

    begin("n", norm_all)
    for i in reversed(range(1, n)):
        send(
            "dn",
            down.at[pl.ds(pl.multiple_of(near(i) * hid + g * half_h, half_h), half_h)],
            down_half(me, g),
            {"sp": near(i)},
            near(i),
            me,
        )

    def raise_block(i):
        z = near(i)
        upward = jnp.dot(norm_all[z].reshape(rows, width), up_all[...], preferred_element_type=f32)
        act[z] = jnp.square(jnp.maximum(upward, 0.0)).astype(bf)

    for i in range(1, n):
        land("uy", up_half(near(i), 1 - g), near(i))
    got_up.wait()
    relay("n", norm_all, 1)
    for i in range(n):
        cross("n", norm_all, i)
        if i + 2 < n:
            relay("n", norm_all, i + 2)
        settle("n", norm_all, i)
        raise_block(i)
    for i in range(1, n):
        piece = down_half(near(i), g)
        land("dn", piece, near(i))
        send("dy", piece, piece, ypeer, near(i), near(i))
    got_down.wait()
    for i in range(1, n):
        land("dy", down_half(near(i), 1 - g), near(i))

    def lower(i):
        dest = near(i)

        @pl.loop(0, width // tile)
        def _(j):
            cols = pl.ds(pl.multiple_of(j * tile, tile), tile)
            made = jnp.dot(act[dest], down_all[:, cols], preferred_element_type=f32)
            part[i, :, :, :, cols] = made.astype(bf).reshape(2, 2, share, tile)

        send(("f1", i), part.at[i, 1 - c], rf1.at[i], sib)

    def fold_core(i):
        land(("f1", i), rf1.at[i])
        c2[i] = (part[i, c, 1 - x].astype(f32) + rf1[i, 1 - x].astype(f32)).astype(bf)
        send(("f2", i), c2.at[i], rf2.at[i], xpeer)

    def fold_x(i):
        land(("f2", i), rf2.at[i])
        c3[i] = (
            part[i, c, x].astype(f32) + rf1[i, x].astype(f32) + rf2[i].astype(f32)
        ).astype(bf)
        if i:
            send("f3", c3.at[i], rf3.at[me], {"sp": near(i)}, near(i), me)

    order = list(reversed(range(n)))
    for at, i in enumerate(order):
        lower(i)
        if at:
            fold_core(order[at - 1])
    fold_core(order[-1])
    for i in order:
        fold_x(i)
    feed = c3[0].astype(f32)
    for i in range(1, n):
        land("f3", rf3.at[near(i)], near(i))
        feed += rf3[near(i)].astype(f32)
    out[...] = (middle[...].astype(f32) + feed).astype(bf)
    for copy in sent:
        copy.wait_send()


def spread_columns(heads):
    head = QUERY_KEY_PLAIN + QUERY_KEY_ROTARY
    half = QUERY_KEY_ROTARY // 2
    unit = QUERY_KEY_PLAIN + VALUE_HEAD_SIZE
    lanes = heads * QUERY_KEY_ROTARY
    perm = np.zeros((heads * head, heads * unit + 2 * lanes), np.float32)
    turn = np.zeros((QUERY_KEY_ROTARY, 2 * lanes), np.float32)
    for h in range(heads):
        for r in range(QUERY_KEY_PLAIN):
            perm[h * head + r, h * unit + r] = 1.0
        for r in range(QUERY_KEY_ROTARY):
            col = h * QUERY_KEY_ROTARY + r
            other, sign = (r + half, -1.0) if r < half else (r - half, 1.0)
            turn[r, col] = 1.0
            turn[other, lanes + col] = sign
            perm[h * head + QUERY_KEY_PLAIN + r, heads * unit + col] = 1.0
            perm[h * head + QUERY_KEY_PLAIN + other, heads * unit + lanes + col] = sign
    return jnp.asarray(perm, jnp.bfloat16), jnp.asarray(turn, jnp.bfloat16)


def run_layer(
    hidden_in, query_latent_rows, key_value_latent, rotary_key, query_norm_gain, key_value_gain,
    query_up_weight, key_value_up_weight, out_proj, feed_gain, feed_up, feed_down, position,
):
    n = lax.axis_size("sp")
    rows, width = hidden_in.shape
    heads = query_up_weight.shape[1] // (QUERY_KEY_PLAIN + QUERY_KEY_ROTARY)
    share = rows // lax.axis_size("tp")
    hid = feed_up.shape[1] // n
    unit = QUERY_KEY_PLAIN + VALUE_HEAD_SIZE
    lanes = heads * QUERY_KEY_ROTARY
    rank = key_value_latent.shape[1]
    bf = jnp.bfloat16
    half = QUERY_KEY_ROTARY // 2
    inverse = 10000.0 ** (-jnp.arange(half, dtype=jnp.float32) * 2.0 / QUERY_KEY_ROTARY)
    angles = position[:, None] * jnp.tile(inverse, lanes // half)[None, :]
    table = jnp.stack([jnp.cos(angles), jnp.sin(angles)])
    perm, turn = spread_columns(heads)
    vmem = pl.BlockSpec(memory_space=pltpu.VMEM)
    anywhere = pl.BlockSpec(memory_space=pl.ANY)
    copies = 24 * n
    block = (share, width)
    return pl.pallas_call(
        lambda *refs: layer_kernel(n, heads, *refs),
        out_shape=jax.ShapeDtypeStruct(block, bf),
        in_specs=[vmem] + [anywhere] * 3 + [vmem] * 4 + [anywhere] * 7,
        out_specs=vmem,
        scratch_shapes=[
            pltpu.VMEM((share, rank), bf),
            pltpu.VMEM((share, rotary_key.shape[1]), bf),
            pltpu.VMEM(query_latent_rows.shape, bf),
            pltpu.VMEM(query_up_weight.shape, bf),
            pltpu.VMEM(key_value_up_weight.shape, bf),
            pltpu.VMEM(perm.shape, bf),
            pltpu.VMEM(block, bf),
            pltpu.VMEM((n, 2, 2, share, rank + lanes), bf),
            pltpu.VMEM((heads, n * rows, unit + lanes), bf),
            pltpu.VMEM((heads, rows, unit + lanes), bf),
            pltpu.VMEM((out_proj.shape[0] * 4, width), bf),
            pltpu.VMEM((heads // 2, rows, unit), bf),
            pltpu.VMEM((share, out_proj.shape[0] * 4), bf),
            pltpu.VMEM((feed_up.shape[0] * n, hid), bf),
            pltpu.VMEM((hid, feed_down.shape[1] * n), bf),
            pltpu.VMEM(block, bf),
            pltpu.VMEM((n, 2, 2, *block), bf),
            pltpu.VMEM((n, rows, hid), bf),
            pltpu.VMEM((n, 2, 2, *block), bf),
            pltpu.VMEM((n, 2, *block), bf),
            pltpu.VMEM((n, *block), bf),
            pltpu.VMEM((n, *block), bf),
            pltpu.VMEM((n, *block), bf),
            pltpu.VMEM((n, *block), bf),
            pltpu.SemaphoreType.DMA((copies,)),
            pltpu.SemaphoreType.DMA((copies,)),
            pltpu.SemaphoreType.DMA((16,)),
        ],
        compiler_params=pltpu.CompilerParams(
            collective_id=0, has_side_effects=True, vmem_limit_bytes=60 * 1024 * 1024
        ),
    )(
        table, key_value_latent, rotary_key, query_latent_rows,
        query_norm_gain.reshape(1, -1), key_value_gain.reshape(1, -1), feed_gain.reshape(1, -1), turn,
        perm, query_up_weight, key_value_up_weight, hidden_in, out_proj, feed_up, feed_down,
    )


def fits_kernel(tokens, query_up_weight, feed_up):
    n = lax.axis_size("sp")
    hid = feed_up.shape[1] // n
    heads = query_up_weight.shape[1] // (QUERY_KEY_PLAIN + QUERY_KEY_ROTARY)
    return (
        lax.axis_size("grp") == 2
        and lax.axis_size("tp") == 4
        and 1 < n
        and tokens * n <= 1024
        and tokens % 64 == 0
        and hid % 128 == 0
        and hid <= 512
        and heads * QUERY_KEY_ROTARY == 128
    )


def on_device(
    hidden_in,
    query_latent_rows,
    key_value_latent,
    rotary_key,
    query_norm_gain,
    key_value_gain,
    query_up_weight,
    key_value_up_weight,
    out_proj,
    feed_gain,
    feed_up,
    feed_down,
):
    tokens_here = hidden_in.shape[0]
    heads_here = query_up_weight.shape[1] // (QUERY_KEY_PLAIN + QUERY_KEY_ROTARY)
    position = (lax.axis_index("sp") * tokens_here + jnp.arange(tokens_here)).astype(jnp.float32)
    if fits_kernel(tokens_here, query_up_weight, feed_up):
        return run_layer(
            hidden_in, query_latent_rows, key_value_latent, rotary_key, query_norm_gain,
            key_value_gain, query_up_weight, key_value_up_weight, out_proj, feed_gain, feed_up,
            feed_down, position,
        )
    scale_factor = (QUERY_KEY_PLAIN + QUERY_KEY_ROTARY) ** (-0.5)
    query_norm = normalize(query_latent_rows, query_norm_gain).astype(jnp.bfloat16)
    queries = jnp.dot(query_norm, query_up_weight, preferred_element_type=jnp.float32).reshape(
        tokens_here, heads_here, QUERY_KEY_PLAIN + QUERY_KEY_ROTARY
    )
    queries = jnp.concatenate(
        [queries[..., :QUERY_KEY_PLAIN], rotate(queries[..., QUERY_KEY_PLAIN:], position)], axis=-1
    ).astype(jnp.bfloat16)
    query_plain = queries[..., :QUERY_KEY_PLAIN]
    query_turned = queries[..., QUERY_KEY_PLAIN:]
    latent = normalize(key_value_latent, key_value_gain).astype(jnp.bfloat16)
    key_rope = rotate(rotary_key.astype(jnp.float32), position).astype(jnp.bfloat16)

    def attend_block(carry, key_plain, value_rows, rope_rows):
        row_max, denom, accum = carry
        scores = jnp.einsum(
            "qhd,khd->hqk", query_plain, key_plain, preferred_element_type=jnp.float32
        )
        scores = scores + jnp.einsum(
            "qhd,kd->hqk", query_turned, rope_rows, preferred_element_type=jnp.float32
        )
        scores = scores * scale_factor
        new_max = jnp.maximum(row_max, jnp.max(scores, axis=-1))
        expo = jnp.exp(scores - new_max[:, :, None])
        factor = jnp.exp(row_max - new_max)
        denom = denom * factor + jnp.sum(expo, axis=-1)
        update = jnp.einsum(
            "hqk,khd->qhd",
            expo.astype(jnp.bfloat16),
            value_rows,
            preferred_element_type=jnp.float32,
        )
        accum = accum * jnp.transpose(factor)[:, :, None] + update
        return (new_max, denom, accum)

    start_carry = (
        jnp.full((heads_here, tokens_here), -1e30, jnp.float32),
        jnp.zeros((heads_here, tokens_here), jnp.float32),
        jnp.zeros((tokens_here, heads_here, VALUE_HEAD_SIZE), jnp.float32),
    )
    own_keys = jnp.dot(latent, key_value_up_weight, preferred_element_type=jnp.float32).astype(
        jnp.bfloat16
    )
    pieces = (
        lax.all_gather(own_keys, "sp", axis=0, tiled=True),
        lax.all_gather(key_rope, "sp", axis=0, tiled=True),
    )
    rows_in = pieces[0].shape[0]
    block = math.gcd(rows_in, 1024)

    def step_block(index, inner):
        first = index * block
        bulk = lax.dynamic_slice_in_dim(pieces[0], first, block, 0)
        rope_rows = lax.dynamic_slice_in_dim(pieces[1], first, block, 0)
        bulk = bulk.reshape(block, heads_here, QUERY_KEY_PLAIN + VALUE_HEAD_SIZE)
        return attend_block(
            inner, bulk[..., :QUERY_KEY_PLAIN], bulk[..., QUERY_KEY_PLAIN:], rope_rows
        )

    final_carry = lax.fori_loop(0, rows_in // block, step_block, start_carry)
    denom = final_carry[1]
    accum = final_carry[2]
    mixed = (
        (accum / jnp.transpose(denom)[:, :, None])
        .astype(jnp.bfloat16)
        .reshape(tokens_here, heads_here * VALUE_HEAD_SIZE)
    )
    up_own = lax.all_to_all(feed_up, "sp", split_axis=1, concat_axis=0, tiled=True)
    down_own = lax.all_to_all(feed_down, "sp", split_axis=0, concat_axis=1, tiled=True)
    share = tokens_here // lax.axis_size("tp")
    lead = lax.axis_index("tp") * share
    branch = lax.psum_scatter(
        jnp.dot(mixed, out_proj, preferred_element_type=jnp.float32).astype(jnp.bfloat16),
        "tp",
        scatter_dimension=0,
        tiled=True,
    ).astype(jnp.float32)
    hidden_own = lax.dynamic_slice_in_dim(hidden_in, lead, share, 0)
    middle_own = (hidden_own.astype(jnp.float32) + branch).astype(jnp.bfloat16)
    normed_own = normalize(middle_own, feed_gain).astype(jnp.bfloat16)
    normed = lax.all_gather(normed_own, ("sp", "tp"), axis=0, tiled=True)
    upward = jnp.dot(normed, up_own, preferred_element_type=jnp.float32)
    activated = jnp.square(jax.nn.relu(upward)).astype(jnp.bfloat16)
    partial_sum = jnp.dot(activated, down_own, preferred_element_type=jnp.float32)
    feed = lax.psum_scatter(
        partial_sum.astype(jnp.bfloat16), ("sp", "tp"), scatter_dimension=0, tiled=True
    ).astype(jnp.float32)
    return (middle_own.astype(jnp.float32) + feed).astype(jnp.bfloat16)


def solution(mesh):
    return jax.shard_map(
        on_device,
        mesh=mesh,
        in_specs=(
            P(("grp", "sp"), None),
            P(("grp", "sp"), None),
            P(("grp", "sp"), None),
            P(("grp", "sp"), None),
            P(),
            P(),
            P(None, "tp"),
            P(None, "tp"),
            P("tp", None),
            P(),
            P("sp", "tp"),
            P("tp", "sp"),
        ),
        out_specs=P(("grp", "sp", "tp"), None),
        check_vma=False,
    )
```

time: 146 us -> 153 us (1.048)
  Pallas kernels: 136 us -> 147 us
  other arithmetic: 3.65 us -> 1.26 us
    pallas_call x1, Pallas kernels: 136 us -> 147 us  [run_layer(): pl.pallas_call(lambda *refs: layer_kernel(n, heads, *refs), out_shape=jax...]
    reduce_sum x2 -> x0, other arithmetic: 2.32 us -> none  [normalize(): jnp.mean(floats * floats, axis=-1, keepdims=True) + 1e-06]
    unnamed x13 -> x2, local copies, waits for them, and re-layouts: 2.06 us -> 3.12 us
where the time goes in v1:
time: 153 us; the launch traced here: 152 us
  Pallas kernels  147 us (96%)
  local copies, waits for them, and re-layouts  4.48 us (3%)
    pallas_call x1, Pallas kernels, run_layer(): pl.pallas_call(lambda *refs: layer_kernel(n, heads, *refs), out_shape=jax...  147 us
    unnamed x2, local copies, waits for them, and re-layouts  3.12 us

profile of v1, /device:TPU:8, one launch (start us, length us, event | category | flops | bytes accessed | tf_op | source)
XLA Modules:
  0.0 152.3 jit_solution(9715812145059734326)
XLA Ops:
  0.0 1.3 reshape.116.refs_4_
  1.3 0.1 mul.33
  1.4 1.4 copy.15.refs_2_
  2.8 0.5 multiply_cosine_fusion
  3.4 0.7 pad_maximum_fusion.refs_0_
  4.1 146.6 %shard_map.136 = bf16[64,2048]{1,0:T(8,128)(2,1)} custom-call(f32[2,256,128]{2,1,0:T(8,128)} %pad_maximum_fusion.refs_0_, bf16[256,512]{1,0:T(8,128)(2,1)} %refs_1_.1, bf16[256,32]{1,0:T(8,128)(2,1)} %copy.15.refs_2_, bf16[256,768]{1,0:T(8,128)(2,1)} %refs_3_.1, f32[1,768]{1,0:T(1,128)} %reshape.116.refs_4_, f32[1,512]{1,0:T(1,128)} %bitcast.3, ...), custom_call_target="tpu_custom_call" | custom-call | tf_op jit(solution)/shard_map/pallas_call | solution.py:398
  150.6 1.7 %copy.17 = bf16[64,2048]{1,0:T(8,128)(2,1)} copy(bf16[64,2048]{1,0:T(8,128)(2,1)} %shard_map.136) | data formatting | bytes 524288
  (3 shorter events, 0.0 us)

commit v2 on v1

--- a/solution.py
+++ b/solution.py
@@ -33,11 +33,12 @@
 
 
 def layer_kernel(
-    n, heads, table, kvlat, rk, qlat, gq, gkv, gain, turn, perm, wq, wkv, hidden, op, up, down, out,
+    heads, table, kvlat, rk, qlat, gq, gkv, gain, turn, perm, wq, wkv, hidden, op, up, down, out,
     lat_in, rk_in, q_in, wq_in, wkv_in, perm_in, hid_in,
-    lat_all, kv_all, q_all, op_all, mixed, mixed_in, up_all, down_all, middle, norm_all, act, part,
-    rf1, c2, rf2, c3, rf3, ss, rs, ls,
+    lat_all, kv_all, q_all, op_chip, mixed, mixed_in, branch_out, branch_in, up_all, down_all, middle,
+    norm_all, act, part, rf1, c2, rf2, c3, near_in, cross_out, cross_in, ss, rs, ls,
 ):
+    n = 4
     g, me, t = lax.axis_index("grp"), lax.axis_index("sp"), lax.axis_index("tp")
     c, x = lax.rem(t, 2), t // 2
     share, width = middle.shape
@@ -52,14 +53,20 @@
     unit = QUERY_KEY_PLAIN + vh
     lanes = heads * QUERY_KEY_ROTARY
     scale_factor = (QUERY_KEY_PLAIN + QUERY_KEY_ROTARY) ** (-0.5)
-    inner = jnp.minimum(me, n - 1 - me)
+    side = me // 2
+    outer = (me == 0) | (me == n - 1)
+    inner = (me == 1) | (me == n - 2)
+    away = 1 - 2 * side
+    partner = me + 1 - 2 * lax.rem(me, 2)
+    edge, gate = side * (n - 1), 1 + side
+    far_edge, far_gate = (1 - side) * (n - 1), 2 - side
 
     def near(i):
         if i == 0:
             return me
-        step = (i + 1) // 2
-        turned = me - step if i % 2 else me + step
-        return jnp.where(i <= 2 * inner, turned, jnp.where(2 * me < n - 1, i, n - 1 - i))
+        if i == 1:
+            return partner
+        return far_gate if i == 2 else far_edge
 
     def at_tp(cc, xx):
         return {"tp": xx * 2 + cc}
@@ -68,13 +75,12 @@
     barrier = pltpu.get_barrier_semaphore()
     for i in range(1, n):
         pl.semaphore_signal(barrier, inc=1, device_id={"sp": near(i)}, device_id_type=MESH)
-    for peer in (sib, xpeer, at_tp(1 - c, 1 - x), ypeer):
+    for peer in (sib, xpeer, ypeer):
         pl.semaphore_signal(barrier, inc=1, device_id=peer, device_id_type=MESH)
 
     def rows_of(tt):
         return pl.ds(pl.multiple_of(tt * share, share), share)
 
-    mine = rows_of(t)
     local = []
 
     def fetch(src, dst):
@@ -83,15 +89,14 @@
         local.append(copy)
         return copy
 
-    got_lat = fetch(kvlat.at[mine], lat_in)
-    got_rk = fetch(rk.at[mine], rk_in)
+    got_lat = fetch(kvlat, lat_in)
+    got_rk = fetch(rk, rk_in)
     got_perm = fetch(perm, perm_in)
     got_wq = fetch(wq, wq_in)
     got_q = fetch(qlat, q_in)
     got_wkv = fetch(wkv, wkv_in)
-    op_rows = op.shape[0]
-    got_op = fetch(op, op_all.at[pl.ds(pl.multiple_of(t * op_rows, op_rows), op_rows)])
-    got_hid = fetch(hidden.at[mine], hid_in)
+    got_op = fetch(op, op_chip.at[c])
+    got_hid = fetch(hidden.at[rows_of(t)], hid_in)
     got_up = fetch(
         up.at[:, pl.ds(pl.multiple_of(me * hid, hid), hid)],
         up_all.at[pl.ds(pl.multiple_of(me * piece_k, piece_k), piece_k)],
@@ -109,13 +114,16 @@
             names[name] = sum(size for _, size in names.values()), 1 if at is None else n
         return names[name][0] + (0 if at is None else at)
 
-    def send(name, src, dst, dev, to=None, by=None):
+    def send(name, src, dst, dev, to=None, by=None, when=None, into=None):
         copy = pltpu.make_async_remote_copy(
-            src_ref=src, dst_ref=dst, send_sem=ss.at[slot(name, to)], recv_sem=rs.at[slot(name, by)],
+            src_ref=src, dst_ref=dst, send_sem=ss.at[slot(name, to)], recv_sem=rs.at[slot(into or name, by)],
             device_id=dev, device_id_type=MESH,
         )
-        copy.start()
-        sent.append(copy)
+        if when is None:
+            copy.start()
+        else:
+            pl.when(when)(copy.start)
+        sent.append((copy, when))
 
     def land(name, dst, by=None):
         pltpu.make_async_remote_copy(
@@ -132,17 +140,9 @@
             pl.ds(pl.multiple_of(owner * wide, wide), wide),
         ]
 
-    def begin(tag, buf):
-        own = buf.at[me, c, x]
-        send((tag, "x"), own, own, xpeer, me, me)
-        for i in reversed(range(1, n)):
-            send((tag, "z"), own, own, {"sp": near(i)}, near(i), me)
-        send((tag, "s"), own, own, sib, me, me)
-
-    def relay(tag, buf, i):
+    def share_on(tag, buf, i):
         z = near(i)
         piece = buf.at[z, c, x]
-        land((tag, "z"), piece, z)
         send((tag, "x"), piece, piece, xpeer, z, z)
         send((tag, "s"), piece, piece, sib, z, z)
 
@@ -157,15 +157,44 @@
         land((tag, "s"), buf.at[z, 1 - c, x], z)
         land((tag, "t"), buf.at[z, 1 - c, 1 - x], z)
 
+    def make_latent(cc, xx):
+        here = rows_of(xx * 2 + cc)
+        lat_all[me, cc, xx, :, :rank] = normalize(lat_in[here, :], gkv[...]).astype(bf)
+        spun = jnp.dot(rk_in[here, :], turn[...], preferred_element_type=f32)
+        lat_all[me, cc, xx, :, rank:] = (
+            spun[:, :lanes] * table[0, here, :] + spun[:, lanes:] * table[1, here, :]
+        ).astype(bf)
+
     got_lat.wait()
     got_rk.wait()
-    lat_all[me, c, x, :, :rank] = normalize(lat_in[...], gkv[...]).astype(bf)
-    spun = jnp.dot(rk_in[...], turn[...], preferred_element_type=f32)
-    lat_all[me, c, x, :, rank:] = (
-        spun[:, :lanes] * table[0, mine, :] + spun[:, lanes:] * table[1, mine, :]
-    ).astype(bf)
-    pl.semaphore_wait(barrier, n + 3)
-    begin("l", lat_all)
+    make_latent(c, x)
+    pl.semaphore_wait(barrier, n + 2)
+    own = lat_all.at[me, c, x]
+    for i in reversed(range(1, n)):
+        send(("l", "z"), own, own, {"sp": near(i)}, near(i), me)
+    got_op.wait()
+    send("os", op_chip.at[c], op_chip.at[c], sib)
+    for cc, xx in ((1 - c, x), (c, 1 - x), (1 - c, 1 - x)):
+        make_latent(cc, xx)
+    got_perm.wait()
+    got_wq.wait()
+    wide_q = jnp.dot(wq_in[...], perm_in[...], preferred_element_type=f32).astype(bf)
+    got_q.wait()
+    query_norm = normalize(q_in[...], gq[...]).astype(bf)
+    spread = jnp.dot(query_norm, wide_q, preferred_element_type=f32)
+    first = heads * unit
+    spin = (
+        spread[:, first : first + lanes] * table[0] + spread[:, first + lanes : first + 2 * lanes] * table[1]
+    )
+    lane = lax.broadcasted_iota(jnp.int32, (rows, lanes), 1)
+    for h in range(heads):
+        q_all[h, :, :unit] = spread[:, h * unit : (h + 1) * unit].astype(bf)
+        keep = (lane >= h * QUERY_KEY_ROTARY) & (lane < (h + 1) * QUERY_KEY_ROTARY)
+        q_all[h, :, unit:] = jnp.where(keep, spin, 0.0).astype(bf)
+
+    for i in range(1, n):
+        land(("l", "z"), lat_all.at[near(i), c, x], near(i))
+        share_on("l", lat_all, i)
     for i in reversed(range(1, n)):
         send(
             "up",
@@ -178,46 +207,10 @@
             near(i),
             me,
         )
-
-    op_parts = 4
-    op_piece = op_rows // op_parts
-
-    def op_block(tt, j):
-        return op_all.at[pl.ds(pl.multiple_of(tt * op_rows + j * op_piece, op_piece), op_piece)]
-
-    def send_op(j):
-        own = op_block(t, j)
-        send(("ox", j), own, own, xpeer)
-
-    got_op.wait()
-    send_op(0)
-    own_op = op_all.at[pl.ds(pl.multiple_of(t * op_rows, op_rows), op_rows)]
-    send("os", own_op, own_op, sib)
-
-    got_perm.wait()
-    got_wq.wait()
-    wide_q = jnp.dot(wq_in[...], perm_in[...], preferred_element_type=f32).astype(bf)
-    got_q.wait()
-    query_norm = normalize(q_in[...], gq[...]).astype(bf)
-    spread = jnp.dot(query_norm, wide_q, preferred_element_type=f32)
-    first = heads * unit
-    spin = (
-        spread[:, first : first + lanes] * table[0] + spread[:, first + lanes : first + 2 * lanes] * table[1]
-    )
-    lane = lax.broadcasted_iota(jnp.int32, (rows, lanes), 1)
-    for h in range(heads):
-        q_all[h, :, :unit] = spread[:, h * unit : (h + 1) * unit].astype(bf)
-        keep = (lane >= h * QUERY_KEY_ROTARY) & (lane < (h + 1) * QUERY_KEY_ROTARY)
-        q_all[h, :, unit:] = jnp.where(keep, spin, 0.0).astype(bf)
-
+    got_wkv.wait()
     for i in range(1, n):
-        relay("l", lat_all, i)
-    for j in range(1, op_parts):
-        send_op(j)
-    got_wkv.wait()
-    for i in range(n):
         cross("l", lat_all, i)
-    for i in range(n):
+    for i in range(1, n):
         settle("l", lat_all, i)
     for j in range(n):
         made = jnp.dot(
@@ -239,47 +232,50 @@
         mix = jnp.dot(expo.astype(bf), kv_all[h, :, :unit], preferred_element_type=f32)
         return mix / total
 
-    others = ((c, 1 - x), (1 - c, 1 - x), (1 - c, x))
+    def head_cols(cc, p):
+        return pl.ds(pl.multiple_of(cc * heads * vh + p * unit, unit), unit)
+
     for p in range(heads // 2):
         left, right = attend(2 * p), attend(2 * p + 1)
         pair = jnp.where(low, pltpu.roll(left, vh, 1), right)
         mixed[p] = pair.astype(bf)
-        cols = pl.ds(pl.multiple_of(t * heads * vh + p * unit, unit), unit)
-        for j, (cc, xx) in enumerate(others):
+        for xx in range(2):
             send(
-                ("m", p, j), mixed.at[p, rows_of(xx * 2 + cc)], mixed_in.at[:, cols], at_tp(cc, xx)
+                ("m", p, xx), mixed.at[p, rows_of(xx * 2 + 1 - c)], mixed_in.at[xx, :, head_cols(c, p)], sib
             )
-        mixed_in[:, cols] = mixed[p, mine, :]
-
-    for j in range(op_parts):
-        piece = op_block((1 - x) * 2 + c, j)
-        land(("ox", j), piece)
-        send(("ot", j), piece, piece, sib)
-    for i in range(1, n):
-        piece = up_half(near(i), g)
-        land("up", piece, near(i))
-        send("uy", piece, piece, ypeer, near(i), near(i))
-    land("os", op_all.at[pl.ds(pl.multiple_of((x * 2 + 1 - c) * op_rows, op_rows), op_rows)])
-    for j in range(op_parts):
-        land(("ot", j), op_block((1 - x) * 2 + 1 - c, j))
+            mixed_in[xx, :, head_cols(c, p)] = mixed[p, rows_of(xx * 2 + c), :]
+
+    land("os", op_chip.at[1 - c])
     for p in range(heads // 2):
-        for j, (cc, xx) in enumerate(others):
-            cols = pl.ds(pl.multiple_of((xx * 2 + cc) * heads * vh + p * unit, unit), unit)
-            land(("m", p, j), mixed_in.at[:, cols])
-
-    tile = math.gcd(width, 512)
+        for xx in range(2):
+            land(("m", p, xx), mixed_in.at[xx, :, head_cols(1 - c, p)])
+
+    tiles = width // wide
+    chip_heads = 2 * heads * vh
+
+    def project(xx, j):
+        return jnp.dot(
+            mixed_in[xx],
+            op_chip[:, :, j * wide : (j + 1) * wide].reshape(chip_heads, wide),
+            preferred_element_type=f32,
+        )
+
+    for j in range(tiles):
+        branch_out[j] = project(1 - x, j).astype(bf)
+        send(("b", j), branch_out.at[j], branch_in.at[j], xpeer)
     got_hid.wait()
-
-    @pl.loop(0, width // tile)
-    def _(j):
-        cols = pl.ds(pl.multiple_of(j * tile, tile), tile)
-        branch = jnp.dot(mixed_in[...], op_all[:, cols], preferred_element_type=f32)
-        middle[:, cols] = (hid_in[:, cols].astype(f32) + branch).astype(bf)
-
+    for j in range(tiles):
+        kept = project(x, j)
+        land(("b", j), branch_in.at[j])
+        cols = slice(j * wide, (j + 1) * wide)
+        middle[:, cols] = (hid_in[:, cols].astype(f32) + (kept + branch_in[j].astype(f32))).astype(bf)
     norm_all[me, c, x] = normalize(middle[...], gain[...]).astype(bf)
 
-    begin("n", norm_all)
-    for i in reversed(range(1, n)):
+    def pass_on(i, to, when):
+        z = near(i)
+        send(("n", "z"), norm_all.at[z, c, x], norm_all.at[z, c, x], {"sp": to}, z, z, when)
+
+    def send_down(i, when):
         send(
             "dn",
             down.at[pl.ds(pl.multiple_of(near(i) * hid + g * half_h, half_h), half_h)],
@@ -287,70 +283,135 @@
             {"sp": near(i)},
             near(i),
             me,
-        )
+            when,
+        )
+
+    own = norm_all.at[me, c, x]
+    send(("n", "z"), own, own, {"sp": partner}, me, me)
+    send(("n", "c"), own, own, {"sp": far_gate}, None, me, inner, ("n", "z"))
+    share_on("n", norm_all, 0)
+    for i in range(1, n):
+        piece = up_half(near(i), g)
+        land("up", piece, near(i))
+        send("uy", piece, piece, ypeer, near(i), near(i))
 
     def raise_block(i):
         z = near(i)
         upward = jnp.dot(norm_all[z].reshape(rows, width), up_all[...], preferred_element_type=f32)
         act[z] = jnp.square(jnp.maximum(upward, 0.0)).astype(bf)
 
+    def relay(i, to):
+        land(("n", "z"), norm_all.at[near(i), c, x], near(i))
+        pass_on(i, to, inner)
+        share_on("n", norm_all, i)
+
+    relay(1, far_gate)
+    send_down(3, inner)
+    send_down(2, inner)
+    cross("n", norm_all, 0)
+    relay(2, partner)
+    for i in reversed(range(1, n)):
+        send_down(i, outer)
     for i in range(1, n):
         land("uy", up_half(near(i), 1 - g), near(i))
     got_up.wait()
-    relay("n", norm_all, 1)
-    for i in range(n):
-        cross("n", norm_all, i)
-        if i + 2 < n:
-            relay("n", norm_all, i + 2)
-        settle("n", norm_all, i)
-        raise_block(i)
-    for i in range(1, n):
-        piece = down_half(near(i), g)
-        land("dn", piece, near(i))
-        send("dy", piece, piece, ypeer, near(i), near(i))
+    settle("n", norm_all, 0)
+    raise_block(0)
+    cross("n", norm_all, 1)
+    relay(3, partner)
+    send_down(1, inner)
+    settle("n", norm_all, 1)
+    raise_block(1)
+    cross("n", norm_all, 2)
+    settle("n", norm_all, 2)
+    raise_block(2)
+    cross("n", norm_all, 3)
+    settle("n", norm_all, 3)
+    raise_block(3)
+
+    def forward(j):
+        piece = down_half(j, g)
+
+        @pl.when(me != j)
+        def _():
+            land("dn", piece, j)
+
+        send("dy", piece, piece, ypeer, j, j, me != j)
+
+    def arrive(j):
+        @pl.when(me != j)
+        def _():
+            land("dy", down_half(j, 1 - g), j)
+
+    def lower(j):
+        @pl.loop(0, n)
+        def _(d):
+            made = jnp.dot(act[d], down_all[:, j * wide : (j + 1) * wide], preferred_element_type=f32)
+            made = made.astype(bf).reshape(2, 2, share, wide)
+            part[j, 0, d] = made[0]
+            part[j, 1, d] = made[1]
+
+        send(("f1", j), part.at[j, 1 - c], rf1.at[j], sib)
+
+    def fold_core(j):
+        land(("f1", j), rf1.at[j])
+        c2[j] = (part[j, c, :, 1 - x].astype(f32) + rf1[j, :, 1 - x].astype(f32)).astype(bf)
+        send(("f2", j), c2.at[j], rf2.at[j], xpeer)
+
+    def fold_x(j):
+        land(("f2", j), rf2.at[j])
+        c3[j] = (
+            part[j, c, :, x].astype(f32) + rf1[j, :, x].astype(f32) + rf2[j].astype(f32)
+        ).astype(bf)
+        send(("pe", j), c3.at[j, far_edge], near_in.at[j, 2], {"sp": partner}, None, None, outer)
+        send(("pg", j), c3.at[j, far_gate], near_in.at[j, 1], {"sp": partner}, None, None, outer)
+        send(("p", j), c3.at[j, partner], near_in.at[j, 0], {"sp": partner})
+
+    def fold_side(j):
+        @pl.when(inner)
+        def _():
+            land(("pe", j), near_in.at[j, 2])
+            cross_out[j, 1] = (c3[j, far_edge].astype(f32) + near_in[j, 2].astype(f32)).astype(bf)
+
+        send(("q", j, 1), cross_out.at[j, 1], cross_in.at[j], {"sp": far_edge}, None, None, inner, ("q", j))
+
+        @pl.when(inner)
+        def _():
+            land(("pg", j), near_in.at[j, 1])
+            cross_out[j, 0] = (c3[j, far_gate].astype(f32) + near_in[j, 1].astype(f32)).astype(bf)
+
+        send(("q", j, 0), cross_out.at[j, 0], cross_in.at[j], {"sp": far_gate}, None, None, inner, ("q", j))
+
+    def finish(j):
+        cols = slice(j * wide, (j + 1) * wide)
+        land(("p", j), near_in.at[j, 0])
+        land(("q", j), cross_in.at[j])
+        feed = c3[j, me].astype(f32) + near_in[j, 0].astype(f32) + cross_in[j].astype(f32)
+        out[:, cols] = (middle[:, cols].astype(f32) + feed).astype(bf)
+
+    order = (1, 2, 0, 3)
+    forward(order[0])
     got_down.wait()
-    for i in range(1, n):
-        land("dy", down_half(near(i), 1 - g), near(i))
-
-    def lower(i):
-        dest = near(i)
-
-        @pl.loop(0, width // tile)
-        def _(j):
-            cols = pl.ds(pl.multiple_of(j * tile, tile), tile)
-            made = jnp.dot(act[dest], down_all[:, cols], preferred_element_type=f32)
-            part[i, :, :, :, cols] = made.astype(bf).reshape(2, 2, share, tile)
-
-        send(("f1", i), part.at[i, 1 - c], rf1.at[i], sib)
-
-    def fold_core(i):
-        land(("f1", i), rf1.at[i])
-        c2[i] = (part[i, c, 1 - x].astype(f32) + rf1[i, 1 - x].astype(f32)).astype(bf)
-        send(("f2", i), c2.at[i], rf2.at[i], xpeer)
-
-    def fold_x(i):
-        land(("f2", i), rf2.at[i])
-        c3[i] = (
-            part[i, c, x].astype(f32) + rf1[i, x].astype(f32) + rf2[i].astype(f32)
-        ).astype(bf)
-        if i:
-            send("f3", c3.at[i], rf3.at[me], {"sp": near(i)}, near(i), me)
-
-    order = list(reversed(range(n)))
-    for at, i in enumerate(order):
-        lower(i)
+    for at, j in enumerate(order):
+        arrive(j)
+        lower(j)
         if at:
-            fold_core(order[at - 1])
-    fold_core(order[-1])
-    for i in order:
-        fold_x(i)
-    feed = c3[0].astype(f32)
-    for i in range(1, n):
-        land("f3", rf3.at[near(i)], near(i))
-        feed += rf3[near(i)].astype(f32)
-    out[...] = (middle[...].astype(f32) + feed).astype(bf)
-    for copy in sent:
-        copy.wait_send()
+            fold_x(order[at - 1])
+        fold_core(j)
+        if at > 1:
+            fold_side(order[at - 2])
+        if at + 1 < n:
+            forward(order[at + 1])
+    fold_x(order[3])
+    fold_side(order[2])
+    fold_side(order[3])
+    for j in order:
+        finish(j)
+    for copy, when in sent:
+        if when is None:
+            copy.wait_send()
+        else:
+            pl.when(when)(copy.wait_send)
 
 
 def spread_columns(heads):
@@ -393,16 +454,17 @@
     perm, turn = spread_columns(heads)
     vmem = pl.BlockSpec(memory_space=pltpu.VMEM)
     anywhere = pl.BlockSpec(memory_space=pl.ANY)
-    copies = 24 * n
+    wide = width // n
+    copies = 32 * n
     block = (share, width)
     return pl.pallas_call(
-        lambda *refs: layer_kernel(n, heads, *refs),
+        lambda *refs: layer_kernel(heads, *refs),
         out_shape=jax.ShapeDtypeStruct(block, bf),
         in_specs=[vmem] + [anywhere] * 3 + [vmem] * 4 + [anywhere] * 7,
         out_specs=vmem,
         scratch_shapes=[
-            pltpu.VMEM((share, rank), bf),
-            pltpu.VMEM((share, rotary_key.shape[1]), bf),
+            pltpu.VMEM(key_value_latent.shape, bf),
+            pltpu.VMEM(rotary_key.shape, bf),
             pltpu.VMEM(query_latent_rows.shape, bf),
             pltpu.VMEM(query_up_weight.shape, bf),
             pltpu.VMEM(key_value_up_weight.shape, bf),
@@ -411,20 +473,24 @@
             pltpu.VMEM((n, 2, 2, share, rank + lanes), bf),
             pltpu.VMEM((heads, n * rows, unit + lanes), bf),
             pltpu.VMEM((heads, rows, unit + lanes), bf),
-            pltpu.VMEM((out_proj.shape[0] * 4, width), bf),
+            pltpu.VMEM((2, *out_proj.shape), bf),
             pltpu.VMEM((heads // 2, rows, unit), bf),
-            pltpu.VMEM((share, out_proj.shape[0] * 4), bf),
+            pltpu.VMEM((2, share, out_proj.shape[0] * 2), bf),
+            pltpu.VMEM((n, share, wide), bf),
+            pltpu.VMEM((n, share, wide), bf),
             pltpu.VMEM((feed_up.shape[0] * n, hid), bf),
-            pltpu.VMEM((hid, feed_down.shape[1] * n), bf),
+            pltpu.VMEM((hid, width), bf),
             pltpu.VMEM(block, bf),
             pltpu.VMEM((n, 2, 2, *block), bf),
             pltpu.VMEM((n, rows, hid), bf),
-            pltpu.VMEM((n, 2, 2, *block), bf),
-            pltpu.VMEM((n, 2, *block), bf),
-            pltpu.VMEM((n, *block), bf),
-            pltpu.VMEM((n, *block), bf),
-            pltpu.VMEM((n, *block), bf),
-            pltpu.VMEM((n, *block), bf),
+            pltpu.VMEM((n, 2, n, 2, share, wide), bf),
+            pltpu.VMEM((n, n, 2, share, wide), bf),
+            pltpu.VMEM((n, n, share, wide), bf),
+            pltpu.VMEM((n, n, share, wide), bf),
+            pltpu.VMEM((n, n, share, wide), bf),
+            pltpu.VMEM((n, 3, share, wide), bf),
+            pltpu.VMEM((n, 2, share, wide), bf),
+            pltpu.VMEM((n, share, wide), bf),
             pltpu.SemaphoreType.DMA((copies,)),
             pltpu.SemaphoreType.DMA((copies,)),
             pltpu.SemaphoreType.DMA((16,)),
@@ -446,7 +512,7 @@
     return (
         lax.axis_size("grp") == 2
         and lax.axis_size("tp") == 4
-        and 1 < n
+        and n == 4
         and tokens * n <= 1024
         and tokens % 64 == 0
         and hid % 128 == 0

time: 153 us -> 142 us (0.928); the launches traced: 152 us -> 140 us
  Pallas kernels: 147 us -> 134 us
    pallas_call x1, Pallas kernels: 147 us -> 134 us  [run_layer(): pl.pallas_call(lambda *refs: layer_kernel(heads, *refs), out_shape=jax.Sh...]
where the time goes in v2:
time: 142 us; the launch traced here: 140 us
  Pallas kernels  134 us (94%)
  local copies, waits for them, and re-layouts  4.48 us (3%)
    pallas_call x1, Pallas kernels, run_layer(): pl.pallas_call(lambda *refs: layer_kernel(heads, *refs), out_shape=jax.Sh...  134 us
    unnamed x2, local copies, waits for them, and re-layouts  3.12 us

profile of v2, /device:TPU:8, one launch (start us, length us, event | category | flops | bytes accessed | tf_op | source)
XLA Modules:
  0.0 139.7 jit_solution(16529034212742561370)
XLA Ops:
  0.0 1.3 reshape.116.refs_4_
  1.3 0.1 mul.33
  1.4 1.4 %copy.15.refs_2_ = bf16[256,32]{1,0:T(8,128)(2,1)} copy(bf16[256,32]{0,1:T(8,128)(2,1)} %param.17) | data formatting | bytes 32768 | tf_op args[3]
  2.8 0.5 multiply_cosine_fusion
  3.4 0.7 pad_maximum_fusion.refs_0_
  4.1 133.9 %shard_map.136 = bf16[64,2048]{1,0:T(8,128)(2,1)} custom-call(f32[2,256,128]{2,1,0:T(8,128)} %pad_maximum_fusion.refs_0_, bf16[256,512]{1,0:T(8,128)(2,1)} %refs_1_.1, bf16[256,32]{1,0:T(8,128)(2,1)} %copy.15.refs_2_, bf16[256,768]{1,0:T(8,128)(2,1)} %refs_3_.1, f32[1,768]{1,0:T(1,128)} %reshape.116.refs_4_, f32[1,512]{1,0:T(1,128)} %bitcast.3, ...), custom_call_target="tpu_custom_call" | custom-call | tf_op jit(solution)/shard_map/pallas_call | solution.py:460
  138.0 1.7 %copy.17 = bf16[64,2048]{1,0:T(8,128)(2,1)} copy(bf16[64,2048]{1,0:T(8,128)(2,1)} %shard_map.136) | data formatting | bytes 524288
  (3 shorter events, 0.0 us)

commit v3 on v2

--- a/solution.py
+++ b/solution.py
@@ -152,9 +152,10 @@
         land((tag, "x"), piece, z)
         send((tag, "t"), piece, piece, sib, z, z)
 
-    def settle(tag, buf, i):
+    def settle(tag, buf, i, both=True):
         z = near(i)
-        land((tag, "s"), buf.at[z, 1 - c, x], z)
+        if both:
+            land((tag, "s"), buf.at[z, 1 - c, x], z)
         land((tag, "t"), buf.at[z, 1 - c, 1 - x], z)
 
     def make_latent(cc, xx):
@@ -192,10 +193,13 @@
         keep = (lane >= h * QUERY_KEY_ROTARY) & (lane < (h + 1) * QUERY_KEY_ROTARY)
         q_all[h, :, unit:] = jnp.where(keep, spin, 0.0).astype(bf)
 
-    for i in range(1, n):
-        land(("l", "z"), lat_all.at[near(i), c, x], near(i))
-        share_on("l", lat_all, i)
-    for i in reversed(range(1, n)):
+    land(("l", "z"), lat_all.at[near(1), c, x], near(1))
+    share_on("l", lat_all, 1)
+    land(("l", "z"), lat_all.at[near(2), c, x], near(2))
+    share_on("l", lat_all, 2)
+    land(("l", "z"), lat_all.at[near(3), c, x], near(3))
+    share_on("l", lat_all, 3)
+    def send_up(i, when):
         send(
             "up",
             up.at[
@@ -206,10 +210,16 @@
             {"sp": near(i)},
             near(i),
             me,
-        )
+            when,
+        )
+
+    send_up(3, inner)
+    send_up(1, None)
     got_wkv.wait()
     for i in range(1, n):
         cross("l", lat_all, i)
+    send_up(3, outer)
+    send_up(2, outer)
     for i in range(1, n):
         settle("l", lat_all, i)
     for j in range(n):
@@ -290,10 +300,18 @@
     send(("n", "z"), own, own, {"sp": partner}, me, me)
     send(("n", "c"), own, own, {"sp": far_gate}, None, me, inner, ("n", "z"))
     share_on("n", norm_all, 0)
-    for i in range(1, n):
+    send_down(1, outer)
+    def forward_up(i, when):
         piece = up_half(near(i), g)
-        land("up", piece, near(i))
-        send("uy", piece, piece, ypeer, near(i), near(i))
+        if when is None:
+            land("up", piece, near(i))
+        else:
+            pl.when(when)(lambda: land("up", piece, near(i)))
+        send("uy", piece, piece, ypeer, near(i), near(i), when)
+
+    forward_up(1, None)
+    forward_up(2, outer)
+    forward_up(3, None)
 
     def raise_block(i):
         z = near(i)
@@ -305,108 +323,129 @@
         pass_on(i, to, inner)
         share_on("n", norm_all, i)
 
+    def forward(i, when):
+        j = near(i)
+        piece = down_half(j, g)
+        if when is None:
+            land("dn", piece, j)
+        else:
+            pl.when(when)(lambda: land("dn", piece, j))
+        send("dy", piece, piece, ypeer, j, j, when)
+
     relay(1, far_gate)
-    send_down(3, inner)
-    send_down(2, inner)
+    send_up(2, inner)
     cross("n", norm_all, 0)
     relay(2, partner)
-    for i in reversed(range(1, n)):
-        send_down(i, outer)
+    cross("n", norm_all, 1)
+    relay(3, partner)
+    land(("n", "s"), norm_all.at[near(3), 1 - c, x], near(3))
+    send_down(2, inner)
+    send_down(3, outer)
+    send_down(2, outer)
+    forward_up(2, inner)
+    cross("n", norm_all, 2)
+    send_down(3, inner)
+    send_down(1, inner)
     for i in range(1, n):
         land("uy", up_half(near(i), 1 - g), near(i))
     got_up.wait()
     settle("n", norm_all, 0)
     raise_block(0)
-    cross("n", norm_all, 1)
-    relay(3, partner)
-    send_down(1, inner)
+    cross("n", norm_all, 3)
     settle("n", norm_all, 1)
     raise_block(1)
-    cross("n", norm_all, 2)
     settle("n", norm_all, 2)
     raise_block(2)
-    cross("n", norm_all, 3)
-    settle("n", norm_all, 3)
+    forward(1, inner)
+    settle("n", norm_all, 3, False)
     raise_block(3)
 
-    def forward(j):
-        piece = down_half(j, g)
-
-        @pl.when(me != j)
-        def _():
-            land("dn", piece, j)
-
-        send("dy", piece, piece, ypeer, j, j, me != j)
-
-    def arrive(j):
-        @pl.when(me != j)
-        def _():
-            land("dy", down_half(j, 1 - g), j)
-
-    def lower(j):
+    def block(j):
+        return pl.ds(pl.multiple_of(j * wide, wide), wide)
+
+    def arrive(i):
+        if i:
+            land("dy", down_half(near(i), 1 - g), near(i))
+        else:
+            got_down.wait()
+
+    def lower(i):
+        j = near(i)
+
         @pl.loop(0, n)
         def _(d):
-            made = jnp.dot(act[d], down_all[:, j * wide : (j + 1) * wide], preferred_element_type=f32)
+            made = jnp.dot(act[d], down_all[:, block(j)], preferred_element_type=f32)
             made = made.astype(bf).reshape(2, 2, share, wide)
             part[j, 0, d] = made[0]
             part[j, 1, d] = made[1]
 
-        send(("f1", j), part.at[j, 1 - c], rf1.at[j], sib)
-
-    def fold_core(j):
-        land(("f1", j), rf1.at[j])
+        send("f1", part.at[j, 1 - c], rf1.at[j], sib, j, j)
+
+    def fold_core(i):
+        j = near(i)
+        land("f1", rf1.at[j], j)
         c2[j] = (part[j, c, :, 1 - x].astype(f32) + rf1[j, :, 1 - x].astype(f32)).astype(bf)
-        send(("f2", j), c2.at[j], rf2.at[j], xpeer)
-
-    def fold_x(j):
-        land(("f2", j), rf2.at[j])
+        send("f2", c2.at[j], rf2.at[j], xpeer, j, j)
+
+    def fold_x(i):
+        j = near(i)
+        land("f2", rf2.at[j], j)
         c3[j] = (
             part[j, c, :, x].astype(f32) + rf1[j, :, x].astype(f32) + rf2[j].astype(f32)
         ).astype(bf)
-        send(("pe", j), c3.at[j, far_edge], near_in.at[j, 2], {"sp": partner}, None, None, outer)
-        send(("pg", j), c3.at[j, far_gate], near_in.at[j, 1], {"sp": partner}, None, None, outer)
-        send(("p", j), c3.at[j, partner], near_in.at[j, 0], {"sp": partner})
-
-    def fold_side(j):
+        send("pe", c3.at[j, far_edge], near_in.at[j, 2], {"sp": partner}, j, j, outer)
+        send("pg", c3.at[j, far_gate], near_in.at[j, 1], {"sp": partner}, j, j, outer)
+        send("p", c3.at[j, partner], near_in.at[j, 0], {"sp": partner}, j, j)
+
+    def fold_side(i):
+        j = near(i)
+
         @pl.when(inner)
         def _():
-            land(("pe", j), near_in.at[j, 2])
+            land("pe", near_in.at[j, 2], j)
             cross_out[j, 1] = (c3[j, far_edge].astype(f32) + near_in[j, 2].astype(f32)).astype(bf)
 
-        send(("q", j, 1), cross_out.at[j, 1], cross_in.at[j], {"sp": far_edge}, None, None, inner, ("q", j))
+        send("q1", cross_out.at[j, 1], cross_in.at[j], {"sp": far_edge}, j, j, inner, "q0")
 
         @pl.when(inner)
         def _():
-            land(("pg", j), near_in.at[j, 1])
+            land("pg", near_in.at[j, 1], j)
             cross_out[j, 0] = (c3[j, far_gate].astype(f32) + near_in[j, 1].astype(f32)).astype(bf)
 
-        send(("q", j, 0), cross_out.at[j, 0], cross_in.at[j], {"sp": far_gate}, None, None, inner, ("q", j))
-
-    def finish(j):
-        cols = slice(j * wide, (j + 1) * wide)
-        land(("p", j), near_in.at[j, 0])
-        land(("q", j), cross_in.at[j])
+        send("q0", cross_out.at[j, 0], cross_in.at[j], {"sp": far_gate}, j, j, inner)
+
+    def finish(i):
+        j = near(i)
+        land("p", near_in.at[j, 0], j)
+        land("q0", cross_in.at[j], j)
         feed = c3[j, me].astype(f32) + near_in[j, 0].astype(f32) + cross_in[j].astype(f32)
-        out[:, cols] = (middle[:, cols].astype(f32) + feed).astype(bf)
-
-    order = (1, 2, 0, 3)
-    forward(order[0])
-    got_down.wait()
-    for at, j in enumerate(order):
-        arrive(j)
-        lower(j)
-        if at:
-            fold_x(order[at - 1])
-        fold_core(j)
-        if at > 1:
-            fold_side(order[at - 2])
-        if at + 1 < n:
-            forward(order[at + 1])
-    fold_x(order[3])
-    fold_side(order[2])
-    fold_side(order[3])
-    for j in order:
-        finish(j)
+        out[:, block(j)] = (middle[:, block(j)].astype(f32) + feed).astype(bf)
+
+    arrive(0)
+    lower(0)
+    fold_core(0)
+    forward(1, outer)
+    forward(2, None)
+    arrive(1)
+    lower(1)
+    fold_core(1)
+    forward(3, None)
+    fold_x(0)
+    arrive(2)
+    lower(2)
+    fold_core(2)
+    fold_x(1)
+    arrive(3)
+    lower(3)
+    fold_core(3)
+    fold_x(2)
+    fold_side(1)
+    fold_side(0)
+    fold_x(3)
+    fold_side(2)
+    fold_side(3)
+    for i in range(n):
+        finish(i)
     for copy, when in sent:
         if when is None:
             copy.wait_send()

time: 142 us -> 114 us (0.80)
  Pallas kernels: 134 us -> 106 us
    pallas_call x1, Pallas kernels: 134 us -> 106 us  [run_layer(): pl.pallas_call(lambda *refs: layer_kernel(heads, *refs), out_shape=jax.Sh...]
where the time goes in v3:
time: 114 us; the launch traced here: 112 us
  Pallas kernels  106 us (93%)
  local copies, waits for them, and re-layouts  4.48 us (4%)
  other arithmetic  1.26 us (1%)
    pallas_call x1, Pallas kernels, run_layer(): pl.pallas_call(lambda *refs: layer_kernel(heads, *refs), out_shape=jax.Sh...  106 us
    unnamed x2, local copies, waits for them, and re-layouts  3.12 us

profile of v3, /device:TPU:8, one launch (start us, length us, event | category | flops | bytes accessed | tf_op | source)
XLA Modules:
  0.0 112.2 jit_solution(17538916885745165569)
XLA Ops:
  0.0 1.3 %reshape.116.refs_4_ = f32[1,768]{1,0:T(1,128)} reshape(f32[768]{0:T(1024)} %param.18) | data formatting | bytes 6144 | tf_op jit(solution)/shard_map/reshape | solution.py:542
  1.3 0.1 mul.33
  1.4 1.4 %copy.15.refs_2_ = bf16[256,32]{1,0:T(8,128)(2,1)} copy(bf16[256,32]{0,1:T(8,128)(2,1)} %param.17) | data formatting | bytes 32768 | tf_op args[3]
  2.8 0.5 multiply_cosine_fusion
  3.4 0.7 pad_maximum_fusion.refs_0_
  4.1 106.4 %shard_map.136 = bf16[64,2048]{1,0:T(8,128)(2,1)} custom-call(f32[2,256,128]{2,1,0:T(8,128)} %pad_maximum_fusion.refs_0_, bf16[256,512]{1,0:T(8,128)(2,1)} %refs_1_.1, bf16[256,32]{1,0:T(8,128)(2,1)} %copy.15.refs_2_, bf16[256,768]{1,0:T(8,128)(2,1)} %refs_3_.1, f32[1,768]{1,0:T(1,128)} %reshape.116.refs_4_, f32[1,512]{1,0:T(1,128)} %bitcast.3, ...), custom_call_target="tpu_custom_call" | custom-call | tf_op jit(solution)/shard_map/pallas_call | solution.py:499
  110.5 1.7 %copy.17 = bf16[64,2048]{1,0:T(8,128)(2,1)} copy(bf16[64,2048]{1,0:T(8,128)(2,1)} %shard_map.136) | data formatting | bytes 524288
  (3 shorter events, 0.0 us)

commit v4 on v3

--- a/solution.py
+++ b/solution.py
@@ -33,8 +33,8 @@
 
 
 def layer_kernel(
-    heads, table, kvlat, rk, qlat, gq, gkv, gain, turn, perm, wq, wkv, hidden, op, up, down, out,
-    lat_in, rk_in, q_in, wq_in, wkv_in, perm_in, hid_in,
+    heads, inverse, turn, kvlat, rk, qlat, gain_q, gain_kv, gain_f, perm, wq, wkv, hidden, op, up, down, out,
+    table, spun, gq, gkv, gain, lat_in, rk_in, q_in, wq_in, wkv_in, perm_in, hid_in,
     lat_all, kv_all, q_all, op_chip, mixed, mixed_in, branch_out, branch_in, up_all, down_all, middle,
     norm_all, act, part, rf1, c2, rf2, c3, near_in, cross_out, cross_in, ss, rs, ls,
 ):
@@ -91,6 +91,9 @@
 
     got_lat = fetch(kvlat, lat_in)
     got_rk = fetch(rk, rk_in)
+    got_gkv = fetch(gain_kv, gkv)
+    got_gq = fetch(gain_q, gq)
+    got_gain = fetch(gain_f, gain)
     got_perm = fetch(perm, perm_in)
     got_wq = fetch(wq, wq_in)
     got_q = fetch(qlat, q_in)
@@ -134,40 +137,71 @@
     def up_half(owner, hv):
         return up_all.at[pl.ds(pl.multiple_of(owner * piece_k + hv * half_k, half_k), half_k)]
 
-    def down_half(owner, hv):
+    part_h = half_h // 2
+
+    def down_half(owner, hv, q):
         return down_all.at[
-            pl.ds(pl.multiple_of(hv * half_h, half_h), half_h),
+            pl.ds(pl.multiple_of(hv * half_h + q * part_h, part_h), part_h),
             pl.ds(pl.multiple_of(owner * wide, wide), wide),
         ]
 
+    def strip(buf, z, cc, xx, tag):
+        if tag[1:] == "":
+            return buf.at[z, cc, xx]
+        deep = share // 2
+        return buf.at[z, cc, xx, int(tag[1:]) * deep : (int(tag[1:]) + 1) * deep]
+
     def share_on(tag, buf, i):
         z = near(i)
-        piece = buf.at[z, c, x]
+        piece = strip(buf, z, c, x, tag)
         send((tag, "x"), piece, piece, xpeer, z, z)
         send((tag, "s"), piece, piece, sib, z, z)
 
-    def cross(tag, buf, i):
+    def cross_one(tag, buf, i):
         z = near(i)
-        piece = buf.at[z, c, 1 - x]
+        piece = strip(buf, z, c, 1 - x, tag)
         land((tag, "x"), piece, z)
         send((tag, "t"), piece, piece, sib, z, z)
+
+    def tags(tag):
+        return ("n0", "n1") if tag == "n" else (tag,)
+
+    def cross(tag, buf, i):
+        for one in tags(tag):
+            cross_one(one, buf, i)
+
+    def land_sib(tag, buf, i):
+        for one in tags(tag):
+            land((one, "s"), strip(buf, near(i), 1 - c, x, one), near(i))
 
     def settle(tag, buf, i, both=True):
         z = near(i)
         if both:
-            land((tag, "s"), buf.at[z, 1 - c, x], z)
-        land((tag, "t"), buf.at[z, 1 - c, 1 - x], z)
+            land_sib(tag, buf, i)
+        for one in tags(tag):
+            land((one, "t"), strip(buf, z, 1 - c, 1 - x, one), z)
 
     def make_latent(cc, xx):
         here = rows_of(xx * 2 + cc)
-        lat_all[me, cc, xx, :, :rank] = normalize(lat_in[here, :], gkv[...]).astype(bf)
-        spun = jnp.dot(rk_in[here, :], turn[...], preferred_element_type=f32)
+        lat_all[me, cc, xx, :, :rank] = normalize(lat_in[here, :], gkv[...].reshape(1, -1)).astype(bf)
         lat_all[me, cc, xx, :, rank:] = (
-            spun[:, :lanes] * table[0, here, :] + spun[:, lanes:] * table[1, here, :]
+            spun[here, :lanes] * table[0, here, :] + spun[here, lanes:] * table[1, here, :]
         ).astype(bf)
 
+    def make_table(tt):
+        here = rows_of(tt)
+        place = lax.broadcasted_iota(jnp.int32, (share, lanes), 0) + (me * rows + tt * share)
+        angle = place.astype(f32) * inverse[...]
+        table[0, here, :] = jnp.cos(angle)
+        table[1, here, :] = jnp.sin(angle)
+
+    make_table(t)
+    got_rk.wait()
+    spun[...] = lax.dot_general(
+        rk_in[...], turn[...], (((0,), (0,)), ((), ())), preferred_element_type=f32
+    )
     got_lat.wait()
-    got_rk.wait()
+    got_gkv.wait()
     make_latent(c, x)
     pl.semaphore_wait(barrier, n + 2)
     own = lat_all.at[me, c, x]
@@ -176,12 +210,14 @@
     got_op.wait()
     send("os", op_chip.at[c], op_chip.at[c], sib)
     for cc, xx in ((1 - c, x), (c, 1 - x), (1 - c, 1 - x)):
+        make_table(xx * 2 + cc)
         make_latent(cc, xx)
     got_perm.wait()
     got_wq.wait()
     wide_q = jnp.dot(wq_in[...], perm_in[...], preferred_element_type=f32).astype(bf)
     got_q.wait()
-    query_norm = normalize(q_in[...], gq[...]).astype(bf)
+    got_gq.wait()
+    query_norm = normalize(q_in[...], gq[...].reshape(1, -1)).astype(bf)
     spread = jnp.dot(query_norm, wide_q, preferred_element_type=f32)
     first = heads * unit
     spin = (
@@ -279,27 +315,31 @@
         land(("b", j), branch_in.at[j])
         cols = slice(j * wide, (j + 1) * wide)
         middle[:, cols] = (hid_in[:, cols].astype(f32) + (kept + branch_in[j].astype(f32))).astype(bf)
-    norm_all[me, c, x] = normalize(middle[...], gain[...]).astype(bf)
-
-    def pass_on(i, to, when):
+    got_gain.wait()
+    norm_all[me, c, x] = normalize(middle[...], gain[...].reshape(1, -1)).astype(bf)
+
+    def pass_on(i, to, when, one):
         z = near(i)
-        send(("n", "z"), norm_all.at[z, c, x], norm_all.at[z, c, x], {"sp": to}, z, z, when)
+        piece = strip(norm_all, z, c, x, one)
+        send((one, "z"), piece, piece, {"sp": to}, z, z, when)
 
     def send_down(i, when):
-        send(
-            "dn",
-            down.at[pl.ds(pl.multiple_of(near(i) * hid + g * half_h, half_h), half_h)],
-            down_half(me, g),
-            {"sp": near(i)},
-            near(i),
-            me,
-            when,
-        )
-
-    own = norm_all.at[me, c, x]
-    send(("n", "z"), own, own, {"sp": partner}, me, me)
-    send(("n", "c"), own, own, {"sp": far_gate}, None, me, inner, ("n", "z"))
-    share_on("n", norm_all, 0)
+        for q in range(2):
+            send(
+                ("dn", q),
+                down.at[pl.ds(pl.multiple_of(near(i) * hid + g * half_h + q * part_h, part_h), part_h)],
+                down_half(me, g, q),
+                {"sp": near(i)},
+                near(i),
+                me,
+                when,
+            )
+
+    for one in tags("n"):
+        own = strip(norm_all, me, c, x, one)
+        send((one, "z"), own, own, {"sp": partner}, me, me)
+        send((one, "c"), own, own, {"sp": far_gate}, None, me, inner, (one, "z"))
+        share_on(one, norm_all, 0)
     send_down(1, outer)
     def forward_up(i, when):
         piece = up_half(near(i), g)
@@ -319,18 +359,20 @@
         act[z] = jnp.square(jnp.maximum(upward, 0.0)).astype(bf)
 
     def relay(i, to):
-        land(("n", "z"), norm_all.at[near(i), c, x], near(i))
-        pass_on(i, to, inner)
-        share_on("n", norm_all, i)
+        for one in tags("n"):
+            land((one, "z"), strip(norm_all, near(i), c, x, one), near(i))
+            pass_on(i, to, inner, one)
+            share_on(one, norm_all, i)
 
     def forward(i, when):
         j = near(i)
-        piece = down_half(j, g)
-        if when is None:
-            land("dn", piece, j)
-        else:
-            pl.when(when)(lambda: land("dn", piece, j))
-        send("dy", piece, piece, ypeer, j, j, when)
+        for q in range(2):
+            piece = down_half(j, g, q)
+            if when is None:
+                land(("dn", q), piece, j)
+            else:
+                pl.when(when)(lambda: land(("dn", q), piece, j))
+            send(("dy", q), piece, piece, ypeer, j, j, when)
 
     relay(1, far_gate)
     send_up(2, inner)
@@ -338,7 +380,7 @@
     relay(2, partner)
     cross("n", norm_all, 1)
     relay(3, partner)
-    land(("n", "s"), norm_all.at[near(3), 1 - c, x], near(3))
+    land_sib("n", norm_all, 3)
     send_down(2, inner)
     send_down(3, outer)
     send_down(2, outer)
@@ -365,7 +407,8 @@
 
     def arrive(i):
         if i:
-            land("dy", down_half(near(i), 1 - g), near(i))
+            for q in range(2):
+                land(("dy", q), down_half(near(i), 1 - g, q), near(i))
         else:
             got_down.wait()
 
@@ -487,23 +530,27 @@
     rank = key_value_latent.shape[1]
     bf = jnp.bfloat16
     half = QUERY_KEY_ROTARY // 2
-    inverse = 10000.0 ** (-jnp.arange(half, dtype=jnp.float32) * 2.0 / QUERY_KEY_ROTARY)
-    angles = position[:, None] * jnp.tile(inverse, lanes // half)[None, :]
-    table = jnp.stack([jnp.cos(angles), jnp.sin(angles)])
+    inverse = 10000.0 ** (-np.arange(half, dtype=np.float32) * 2.0 / QUERY_KEY_ROTARY)
+    inverse = jnp.asarray(np.tile(inverse, lanes // half)[None, :], jnp.float32)
     perm, turn = spread_columns(heads)
     vmem = pl.BlockSpec(memory_space=pltpu.VMEM)
     anywhere = pl.BlockSpec(memory_space=pl.ANY)
     wide = width // n
-    copies = 32 * n
+    copies = 28 * n
     block = (share, width)
     return pl.pallas_call(
         lambda *refs: layer_kernel(heads, *refs),
-        out_shape=jax.ShapeDtypeStruct(block, bf),
-        in_specs=[vmem] + [anywhere] * 3 + [vmem] * 4 + [anywhere] * 7,
+        out_shape=pltpu.VMEM(block, bf),
+        in_specs=[vmem] * 2 + [anywhere] * 13,
         out_specs=vmem,
         scratch_shapes=[
+            pltpu.VMEM((2, rows, lanes), jnp.float32),
+            pltpu.VMEM((rows, 2 * lanes), jnp.float32),
+            pltpu.VMEM(query_norm_gain.shape, jnp.float32),
+            pltpu.VMEM(key_value_gain.shape, jnp.float32),
+            pltpu.VMEM(feed_gain.shape, jnp.float32),
             pltpu.VMEM(key_value_latent.shape, bf),
-            pltpu.VMEM(rotary_key.shape, bf),
+            pltpu.VMEM(rotary_key.T.shape, bf),
             pltpu.VMEM(query_latent_rows.shape, bf),
             pltpu.VMEM(query_up_weight.shape, bf),
             pltpu.VMEM(key_value_up_weight.shape, bf),
@@ -538,9 +585,9 @@
             collective_id=0, has_side_effects=True, vmem_limit_bytes=60 * 1024 * 1024
         ),
     )(
-        table, key_value_latent, rotary_key, query_latent_rows,
-        query_norm_gain.reshape(1, -1), key_value_gain.reshape(1, -1), feed_gain.reshape(1, -1), turn,
-        perm, query_up_weight, key_value_up_weight, hidden_in, out_proj, feed_up, feed_down,
+        inverse, turn, key_value_latent, rotary_key.T, query_latent_rows, query_norm_gain,
+        key_value_gain, feed_gain, perm, query_up_weight, key_value_up_weight, hidden_in, out_proj,
+        feed_up, feed_down,
     )
 
 

time: 114 us -> 105 us (0.921)
  local copies, waits for them, and re-layouts: 4.48 us -> 0.71 us
  Pallas kernels: 106 us -> 103 us
  other arithmetic: 1.26 us -> 0 us
    pallas_call x1, Pallas kernels: 106 us -> 103 us  [run_layer(): pl.pallas_call(lambda *refs: layer_kernel(heads, *refs), out_shape=pltpu....]
    unnamed x2 -> x1, local copies, waits for them, and re-layouts: 3.12 us -> 0.71 us
    reshape x1 -> x0, local copies, waits for them, and re-layouts: 1.28 us -> none  [run_layer(): query_norm_gain.reshape(1, -1)]
where the time goes in v4:
time: 105 us; the launch traced here: 104 us
  Pallas kernels  103 us (98%)
    pallas_call x1, Pallas kernels, run_layer(): pl.pallas_call(lambda *refs: layer_kernel(heads, *refs), out_shape=pltpu....  103 us

profile of v4, /device:TPU:8, one launch (start us, length us, event | category | flops | bytes accessed | tf_op | source)
XLA Modules:
  0.0 103.6 jit_solution(11079874964193916083)
XLA Ops:
  0.0 102.9 %shard_map.145 = bf16[64,2048]{1,0:T(8,128)(2,1)S(1)} custom-call(f32[1,128]{1,0:T(1,128)} %constant.6.clone.refs_0_, bf16[32,256]{1,0:T(8,128)(2,1)} %constant.8.clone.refs_1_, bf16[256,512]{1,0:T(8,128)(2,1)} %refs_2_.1, bf16[32,256]{1,0:T(8,128)(2,1)} %bitcast.1, bf16[256,768]{1,0:T(8,128)(2,1)} %refs_4_.1, f32[768]{0:T(1024)} %refs_5_.1, f32[512]{0:T(512)} %refs_6_.1, ...), custom_call_target="tpu_custom_call" | custom-call | tf_op jit(solution)/shard_map/pallas_call | solution.py:541
  102.9 0.7 copy.17

commit v5 on v4

--- a/solution.py
+++ b/solution.py
@@ -205,7 +205,7 @@
     make_latent(c, x)
     pl.semaphore_wait(barrier, n + 2)
     own = lat_all.at[me, c, x]
-    for i in reversed(range(1, n)):
+    for i in reversed(range(1, 3)):
         send(("l", "z"), own, own, {"sp": near(i)}, near(i), me)
     got_op.wait()
     send("os", op_chip.at[c], op_chip.at[c], sib)
@@ -229,11 +229,17 @@
         keep = (lane >= h * QUERY_KEY_ROTARY) & (lane < (h + 1) * QUERY_KEY_ROTARY)
         q_all[h, :, unit:] = jnp.where(keep, spin, 0.0).astype(bf)
 
+    def hand_on(i):
+        piece = lat_all.at[near(i), c, x]
+        send(("l", "r"), piece, piece, {"sp": partner}, near(i), near(i), inner, ("l", "z"))
+
     land(("l", "z"), lat_all.at[near(1), c, x], near(1))
     share_on("l", lat_all, 1)
     land(("l", "z"), lat_all.at[near(2), c, x], near(2))
+    hand_on(2)
     share_on("l", lat_all, 2)
     land(("l", "z"), lat_all.at[near(3), c, x], near(3))
+    hand_on(3)
     share_on("l", lat_all, 3)
     def send_up(i, when):
         send(
@@ -249,13 +255,14 @@
             when,
         )
 
-    send_up(3, inner)
-    send_up(1, None)
+    send_up(2, inner)
+    send_up(1, outer)
     got_wkv.wait()
     for i in range(1, n):
         cross("l", lat_all, i)
-    send_up(3, outer)
+    send_up(3, None)
     send_up(2, outer)
+    send_up(1, inner)
     for i in range(1, n):
         settle("l", lat_all, i)
     for j in range(n):
@@ -350,7 +357,7 @@
         send("uy", piece, piece, ypeer, near(i), near(i), when)
 
     forward_up(1, None)
-    forward_up(2, outer)
+    forward_up(2, None)
     forward_up(3, None)
 
     def raise_block(i):
@@ -375,7 +382,6 @@
             send(("dy", q), piece, piece, ypeer, j, j, when)
 
     relay(1, far_gate)
-    send_up(2, inner)
     cross("n", norm_all, 0)
     relay(2, partner)
     cross("n", norm_all, 1)
@@ -384,7 +390,6 @@
     send_down(2, inner)
     send_down(3, outer)
     send_down(2, outer)
-    forward_up(2, inner)
     cross("n", norm_all, 2)
     send_down(3, inner)
     send_down(1, inner)
@@ -536,7 +541,7 @@
     vmem = pl.BlockSpec(memory_space=pltpu.VMEM)
     anywhere = pl.BlockSpec(memory_space=pl.ANY)
     wide = width // n
-    copies = 28 * n
+    copies = 29 * n
     block = (share, width)
     return pl.pallas_call(
         lambda *refs: layer_kernel(heads, *refs),

time: 105 us -> 105 us (level)
  no operation moved by 1% of the time
where the time goes in v5:
time: 105 us; the launch traced here: 103 us
  Pallas kernels  102 us (97%)
    pallas_call x1, Pallas kernels, run_layer(): pl.pallas_call(lambda *refs: layer_kernel(heads, *refs), out_shape=pltpu....  102 us

profile of v5, /device:TPU:8, one launch (start us, length us, event | category | flops | bytes accessed | tf_op | source)
XLA Modules:
  0.0 103.0 jit_solution(12315364051000196737)
XLA Ops:
  0.0 102.3 %shard_map.145 = bf16[64,2048]{1,0:T(8,128)(2,1)S(1)} custom-call(f32[1,128]{1,0:T(1,128)} %constant.6.clone.refs_0_, bf16[32,256]{1,0:T(8,128)(2,1)} %constant.8.clone.refs_1_, bf16[256,512]{1,0:T(8,128)(2,1)} %refs_2_.1, bf16[32,256]{1,0:T(8,128)(2,1)} %bitcast.1, bf16[256,768]{1,0:T(8,128)(2,1)} %refs_4_.1, f32[768]{0:T(1024)} %refs_5_.1, f32[512]{0:T(512)} %refs_6_.1, ...), custom_call_target="tpu_custom_call" | custom-call | tf_op jit(solution)/shard_map/pallas_call | solution.py:546
  102.3 0.7 copy.17
